TPU v7x, 32 devices: a whole 2x2x4 slice. The times are simulated.
32 devices in a mesh: dp: 4 (over y, x), kv: 4 (over z), tp: 2 (over core).
Axes of the slice: x: 2, y: 2, z: 4, core: 2. Of those that a mesh axis runs over, the one named last changes fastest.
Arguments:
- tokens: bfloat16 [4096, 2048], P(('dp', 'kv'), 'tp'), parts along dimension 0, may hold values from -6 to 6
- query_weight: bfloat16 [2048, 1024], P(None, 'tp'), may hold values from -2 to 2
- key_weight: bfloat16 [2048, 1024], P(None, 'tp'), may hold values from -2 to 2
- value_weight: bfloat16 [2048, 1024], P(None, 'tp'), may hold values from -0.125 to 0.125
- out_weight: bfloat16 [1024, 2048], P(None, 'tp'), may hold values from -0.75 to 0.75
- chosen: int32 [128, 16], P(('dp', 'kv')), parts along dimension 0, may hold values from -1 to 31, as said below
Outputs:
- mixed: bfloat16 [4096, 2048], P(('dp', 'kv'), 'tp'), parts along dimension 0
There are 4 independent parts, one for each index of `dp`. A program takes and returns all parts, laid end to end along the dimension named above; an argument that names none is the same for every part. Nothing has to cross between parts.
Inputs may be any that keep to these rules, and one draw needn't show every extreme that they name: Each row of chosen lists distinct key blocks no later than its own query block, followed or mixed with -1 for empty slots; the own block is always listed, and block 0 too. For the 8 query blocks of one index of kv (aligned runs of rows), the distinct listed key blocks that lie among the 8 blocks of any one other index number at most 3, and exactly 3 for the index just before.
All inputs are finite; a program needn't handle non-finite values.
Results may differ from a plain program's by a relative error of at most 0.0084.
Values may be sent and summed in bfloat16 or wider, within the bound.
No kernel may reach another device: no remote copies, remote signals or barrier semaphores. Data moves between devices by JAX's collectives and lax.ppermute only.
A program may use at most 128 MiB of HBM per device.

v0:
```python
import jax
import jax.numpy as jnp
from jax import lax
from jax.sharding import PartitionSpec as P

HEAD_DIM = 64
BLOCK = 32
CAP = 3


rotary_base = 500000.0
masked_score = -1e30


def rotate(heads_in, positions):
    half_dim = heads_in.shape[-1] // 2
    inverse = 1.0 / rotary_base ** (jnp.arange(half_dim, dtype=jnp.float32) / half_dim)
    angles = positions.astype(jnp.float32)[:, None] * inverse[None, :]
    cosine = jnp.cos(angles)[:, None, :]
    sine_part = jnp.sin(angles)[:, None, :]
    first_half = heads_in[..., :half_dim]
    second_half = heads_in[..., half_dim:]
    return jnp.concatenate(
        [
            first_half * cosine - second_half * sine_part,
            first_half * sine_part + second_half * cosine,
        ],
        axis=-1,
    )


def attend_keys(
    carried, queries, key_rows, value_rows, key_block, key_pos, key_valid, listed, query_pos
):
    key_count = key_rows.shape[0]
    head_count = queries.shape[0]
    hit_mask = jnp.any(listed[:, :, None] == key_block[None, None, :], axis=1)
    hit_mask = jnp.repeat(hit_mask, BLOCK, axis=0)
    allowed = hit_mask & key_valid[None, :] & (key_pos[None, :] <= query_pos[:, None])
    keys_heads = key_rows.reshape(key_count, head_count, HEAD_DIM).transpose(1, 0, 2)
    values_heads = value_rows.reshape(key_count, head_count, HEAD_DIM).transpose(1, 0, 2)
    score_scale = HEAD_DIM ** (-0.5)

    def one_head(inputs):
        query_head, key_head, value_head, peak_now, denominator, summed = inputs
        scores = (
            jnp.einsum("qd,kd->qk", query_head, key_head, preferred_element_type=jnp.float32)
            * score_scale
        )
        scores = jnp.where(allowed, scores, masked_score)
        peak_new = jnp.maximum(peak_now, jnp.max(scores, axis=1))
        factor = jnp.exp(peak_now - peak_new)
        weights = jnp.where(allowed, jnp.exp(scores - peak_new[:, None]), 0.0)
        denominator = denominator * factor + jnp.sum(weights, axis=1)
        summed = summed * factor[:, None] + jnp.dot(
            weights.astype(jnp.bfloat16), value_head, preferred_element_type=jnp.float32
        )
        return (peak_new, denominator, summed)

    peak_now, denominator, summed = carried
    return lax.map(one_head, (queries, keys_heads, values_heads, peak_now, denominator, summed))


def on_device(tokens, query_weight, key_weight, value_weight, out_weight, chosen):
    row_count = tokens.shape[0]
    head_width = query_weight.shape[1]
    head_count = head_width // HEAD_DIM
    device = lax.axis_index("kv")
    devices = lax.axis_size("kv")
    blocks_dev = row_count // BLOCK
    query_pos = device * row_count + jnp.arange(row_count, dtype=jnp.int32)
    fragment = lax.all_gather(tokens, "tp", axis=1, tiled=True)
    query_acc, key_acc, value_acc = tuple(
        (
            jnp.dot(fragment, weight, preferred_element_type=jnp.float32)
            for weight in (query_weight, key_weight, value_weight)
        )
    )
    heads_shape = (row_count, head_count, HEAD_DIM)
    query_proj = rotate(query_acc.reshape(heads_shape), query_pos).astype(jnp.bfloat16)
    key_proj = (
        rotate(key_acc.reshape(heads_shape), query_pos)
        .astype(jnp.bfloat16)
        .reshape(row_count, head_width)
    )
    value_proj = value_acc.astype(jnp.bfloat16)
    queries = query_proj.transpose(1, 0, 2)
    start_state = (
        jnp.full((head_count, row_count), masked_score, jnp.float32),
        jnp.zeros((head_count, row_count), jnp.float32),
        jnp.zeros((head_count, row_count, HEAD_DIM), jnp.float32),
    )
    block_ids = jnp.arange(devices * blocks_dev, dtype=jnp.int32)
    needed = jnp.any(chosen.reshape(-1)[:, None] == block_ids[None, :], axis=0)
    needed = needed & (block_ids // blocks_dev != device)
    need_grid = needed.reshape(devices, blocks_dev).astype(jnp.int32)
    rank_in = jnp.cumsum(need_grid, axis=1) - need_grid
    slot_hit = (need_grid[:, None, :] == 1) & (
        rank_in[:, None, :] == jnp.arange(CAP, dtype=jnp.int32)[None, :, None]
    )
    request = jnp.sum(
        slot_hit.astype(jnp.int32) * jnp.arange(blocks_dev, dtype=jnp.int32)[None, None, :], axis=2
    )
    present = jnp.any(slot_hit, axis=2)
    incoming = lax.all_to_all(request, "kv", split_axis=0, concat_axis=0, tiled=True)
    key_store = key_proj.reshape(blocks_dev, BLOCK, head_width)
    value_store = value_proj.reshape(blocks_dev, BLOCK, head_width)
    got_keys, got_values = (
        lax.all_to_all(key_store[incoming], "kv", split_axis=0, concat_axis=0, tiled=True),
        lax.all_to_all(value_store[incoming], "kv", split_axis=0, concat_axis=0, tiled=True),
    )
    remote_block = jnp.arange(devices, dtype=jnp.int32)[:, None] * blocks_dev + request
    remote_pos = (
        remote_block[:, :, None] * BLOCK + jnp.arange(BLOCK, dtype=jnp.int32)[None, None, :]
    ).reshape(-1)
    remote_valid = jnp.broadcast_to(present[:, :, None], (devices, CAP, BLOCK)).reshape(-1)
    key_rows = jnp.concatenate([key_proj, got_keys.reshape(-1, head_width)], axis=0)
    value_rows = jnp.concatenate([value_proj, got_values.reshape(-1, head_width)], axis=0)
    key_pos = jnp.concatenate([query_pos, remote_pos])
    key_valid = jnp.concatenate([jnp.ones((row_count,), jnp.bool_), remote_valid])
    peak_now, denominator, summed = attend_keys(
        start_state,
        queries,
        key_rows,
        value_rows,
        key_pos // BLOCK,
        key_pos,
        key_valid,
        chosen,
        query_pos,
    )
    attended = (
        (summed / denominator[:, :, None])
        .astype(jnp.bfloat16)
        .transpose(1, 0, 2)
        .reshape(row_count, head_width)
    )
    mixed = jnp.dot(
        lax.all_gather(attended, "tp", axis=1, tiled=True),
        out_weight,
        preferred_element_type=jnp.float32,
    )
    return mixed.astype(jnp.bfloat16)


def solution(mesh):
    placed = (
        P(("dp", "kv"), "tp"),
        P(None, "tp"),
        P(None, "tp"),
        P(None, "tp"),
        P(None, "tp"),
        P(("dp", "kv"), None),
    )
    return jax.shard_map(
        on_device, mesh=mesh, in_specs=placed, out_specs=P(("dp", "kv"), "tp"), check_vma=False
    )
```

profile of v0, /device:TPU:0, one launch (start us, length us, event | category | flops | bytes accessed | tf_op | source)
XLA Modules:
  0.0 97.7 jit_solution(7026933683414445117)
XLA Ops:
  9.3 6.3 %all-to-all-start = ((s32[4,1,3]{2,1,0:T(1,128)}), s32[4,1,3]{2,1,0:T(1,128)S(1)}, u32[]{:S(2)}, u32[]{:S(2)}) async-start(s32[4,1,3]{2,1,0:T(1,128)} %copy.41), calls=%async_computation | async-start | bytes 4096 | tf_op jit(solution)/shard_map/all_to_all | solution.py:105
  16.0 5.1 %all-to-all-done = s32[4,1,3]{2,1,0:T(1,128)S(1)} async-done(((s32[4,1,3]{2,1,0:T(1,128)}), s32[4,1,3]{2,1,0:T(1,128)S(1)}, u32[]{:S(2)}, u32[]{:S(2)}) %all-to-all-start) | async-done | bytes 80 | tf_op jit(solution)/shard_map/all_to_all | solution.py:105
  21.4 2.8 %fusion.36 = f32[256,512]{0,1:T(8,128)S(1)} fusion(bf16[256,2048]{1,0:T(8,128)(2,1)} %all-gather.2.cloned.1.call-done, bf16[2048,512]{1,0:T(8,128)(2,1)} %param.10), kind=kOutput, calls=%fused_computation.78 | convolution fusion | flops 536870912 | bytes 3670016 | tf_op jit(solution)/shard_map/dot_general | solution.py:75
  25.1 1.3 %gather_fusion = bf16[12,32,512]{2,1,0:T(8,128)(2,1)} fusion(bf16[8,32,512]{2,1,0:T(8,128)(2,1)S(1)} %convert_element_type.47, s32[1024]{0:T(1024)S(1)} %pad_clamp_fusion), kind=kCustom, calls=%fused_computation | custom fusion | bytes 786480 | tf_op jit(solution)/shard_map/gather | solution.py:109
  26.4 4.1 %all-to-all-start.1 = ((bf16[4,3,32,512]{3,2,1,0:T(8,128)(2,1)}), bf16[4,3,32,512]{3,2,1,0:T(8,128)(2,1)S(1)}, u32[]{:S(2)}, u32[]{:S(2)}) async-start(bf16[4,3,32,512]{3,2,1,0:T(8,128)(2,1)} %bitcast.5), calls=%async_computation.1 | async-start | bytes 786432 | tf_op jit(solution)/shard_map/all_to_all | solution.py:109
  31.8 2.6 %convolution_convert_fusion.1 = bf16[256,512]{1,0:T(8,128)(2,1)S(1)} fusion(bf16[256,2048]{1,0:T(8,128)(2,1)} %all-gather.2.cloned.1.call-done, bf16[2048,512]{1,0:T(8,128)(2,1)} %param.11), kind=kOutput, calls=%fused_computation.30 | convolution fusion | flops 537001984 | bytes 3407872 | tf_op jit(solution)/shard_map/dot_general | solution.py:75
  34.4 1.3 %gather_fusion.1 = bf16[12,32,512]{2,1,0:T(8,128)(2,1)} fusion(bf16[8,32,512]{2,1,0:T(8,128)(2,1)S(1)} %bitcast.71, s32[1024]{0:T(1024)S(1)} %pad_clamp_fusion), kind=kCustom, calls=%fused_computation.1 | custom fusion | bytes 786480 | tf_op jit(solution)/shard_map/gather | solution.py:110
  35.8 6.9 %all-to-all-done.1 = bf16[4,3,32,512]{3,2,1,0:T(8,128)(2,1)S(1)} async-done(((bf16[4,3,32,512]{3,2,1,0:T(8,128)(2,1)}), bf16[4,3,32,512]{3,2,1,0:T(8,128)(2,1)S(1)}, u32[]{:S(2)}, u32[]{:S(2)}) %all-to-all-start.1) | async-done | bytes 393248 | tf_op jit(solution)/shard_map/all_to_all | solution.py:109
  42.7 4.1 %all-to-all-start.2 = ((bf16[4,3,32,512]{3,2,1,0:T(8,128)(2,1)}), bf16[4,3,32,512]{3,2,1,0:T(8,128)(2,1)}, u32[]{:S(2)}, u32[]{:S(2)}) async-start(bf16[4,3,32,512]{3,2,1,0:T(8,128)(2,1)} %bitcast.9), calls=%async_computation.2 | async-start | bytes 786432 | tf_op jit(solution)/shard_map/all_to_all | solution.py:110
  46.8 3.6 %fusion.35 = f32[256,512]{0,1:T(8,128)} fusion(bf16[256,2048]{1,0:T(8,128)(2,1)} %all-gather.2.cloned.1.call-done, bf16[2048,512]{1,0:T(8,128)(2,1)} %param.9), kind=kOutput, calls=%fused_computation.77 | convolution fusion | flops 536870912 | bytes 3670016 | tf_op jit(solution)/shard_map/dot_general | solution.py:75
  53.5 1.5 %concatenate.42 = bf16[384,8,64]{2,1,0:T(8,128)(2,1)S(1)} reshape(bf16[4,3,32,512]{3,2,1,0:T(8,128)(2,1)} %copy-done.2) | data formatting | bytes 786432 | tf_op jit(solution)/shard_map/concatenate | solution.py:117
  56.6 1.6 %all-to-all-done.2 = bf16[4,3,32,512]{3,2,1,0:T(8,128)(2,1)} async-done(((bf16[4,3,32,512]{3,2,1,0:T(8,128)(2,1)}), bf16[4,3,32,512]{3,2,1,0:T(8,128)(2,1)}, u32[]{:S(2)}, u32[]{:S(2)}) %all-to-all-start.2) | async-done | bytes 393248 | tf_op jit(solution)/shard_map/all_to_all | solution.py:110
  58.1 1.5 %concatenate.47 = bf16[384,8,64]{2,1,0:T(8,128)(2,1)S(1)} reshape(bf16[4,3,32,512]{3,2,1,0:T(8,128)(2,1)} %all-to-all-done.2) | data formatting | bytes 786432 | tf_op jit(solution)/shard_map/concatenate | solution.py:118
  61.3 25.8 %while.13 = (s32[]{:T(128)}, f32[8,256]{1,0:T(8,128)S(1)}, f32[8,256,64]{1,2,0:T(8,128)S(1)}, bf16[8,256,64]{1,2,0:T(8,128)(2,1)}, bf16[8,640,64]{2,1,0:T(8,128)...) while((s32[]{:T(128)}, f32[8,256]{1,0:T(8,128)S(1)}, ...), condition=%wide.region_8.9_spmd.clone, body=%wide.region_5.8_spmd.clone.sunk | while | flops 44417792 | bytes 2917761 | solution.py:61
  61.5 1.3 %fusion.54 = (f32[256]{0:T(256)S(1)}, f32[256,640]{1,0:T(8,128)S(1)}) fusion(pred[256,640]{1,0:T(32,128)(4,1)S(1)} %fusion.53, bf16[8,640,64]{2,1,0:T(8,128)(2,1)} %get-tuple-element.234, s32[]{:T(128)S(6)} %copy.62, bf16[8,256,64]{1,2,0:T(8,128)(2,1)} %get-tuple-element.233), kind=kOutput, calls=%fused_computation.76.clone.1 | convolution fusion | flops 21462784 | bytes 1017856 | tf_op jit(solution)/shard_map/while/body/eval_jaxpr/qd,kd->qk/dot_general | solution.py:47
  64.7 1.3 %fusion.54 = (f32[256]{0:T(256)S(1)}, f32[256,640]{1,0:T(8,128)S(1)}) fusion(pred[256,640]{1,0:T(32,128)(4,1)S(1)} %fusion.53, bf16[8,640,64]{2,1,0:T(8,128)(2,1)} %get-tuple-element.234, s32[]{:T(128)S(6)} %copy.62, bf16[8,256,64]{1,2,0:T(8,128)(2,1)} %get-tuple-element.233), kind=kOutput, calls=%fused_computation.76.clone.1 | convolution fusion | flops 21462784 | bytes 1017856 | tf_op jit(solution)/shard_map/while/body/eval_jaxpr/qd,kd->qk/dot_general | solution.py:47
  67.9 1.3 %fusion.54 = (f32[256]{0:T(256)S(1)}, f32[256,640]{1,0:T(8,128)S(1)}) fusion(pred[256,640]{1,0:T(32,128)(4,1)S(1)} %fusion.53, bf16[8,640,64]{2,1,0:T(8,128)(2,1)} %get-tuple-element.234, s32[]{:T(128)S(6)} %copy.62, bf16[8,256,64]{1,2,0:T(8,128)(2,1)} %get-tuple-element.233), kind=kOutput, calls=%fused_computation.76.clone.1 | convolution fusion | flops 21462784 | bytes 1017856 | tf_op jit(solution)/shard_map/while/body/eval_jaxpr/qd,kd->qk/dot_general | solution.py:47
  71.1 1.3 %fusion.54 = (f32[256]{0:T(256)S(1)}, f32[256,640]{1,0:T(8,128)S(1)}) fusion(pred[256,640]{1,0:T(32,128)(4,1)S(1)} %fusion.53, bf16[8,640,64]{2,1,0:T(8,128)(2,1)} %get-tuple-element.234, s32[]{:T(128)S(6)} %copy.62, bf16[8,256,64]{1,2,0:T(8,128)(2,1)} %get-tuple-element.233), kind=kOutput, calls=%fused_computation.76.clone.1 | convolution fusion | flops 21462784 | bytes 1017856 | tf_op jit(solution)/shard_map/while/body/eval_jaxpr/qd,kd->qk/dot_general | solution.py:47
  74.4 1.3 %fusion.54 = (f32[256]{0:T(256)S(1)}, f32[256,640]{1,0:T(8,128)S(1)}) fusion(pred[256,640]{1,0:T(32,128)(4,1)S(1)} %fusion.53, bf16[8,640,64]{2,1,0:T(8,128)(2,1)} %get-tuple-element.234, s32[]{:T(128)S(6)} %copy.62, bf16[8,256,64]{1,2,0:T(8,128)(2,1)} %get-tuple-element.233), kind=kOutput, calls=%fused_computation.76.clone.1 | convolution fusion | flops 21462784 | bytes 1017856 | tf_op jit(solution)/shard_map/while/body/eval_jaxpr/qd,kd->qk/dot_general | solution.py:47
  77.6 1.3 %fusion.54 = (f32[256]{0:T(256)S(1)}, f32[256,640]{1,0:T(8,128)S(1)}) fusion(pred[256,640]{1,0:T(32,128)(4,1)S(1)} %fusion.53, bf16[8,640,64]{2,1,0:T(8,128)(2,1)} %get-tuple-element.234, s32[]{:T(128)S(6)} %copy.62, bf16[8,256,64]{1,2,0:T(8,128)(2,1)} %get-tuple-element.233), kind=kOutput, calls=%fused_computation.76.clone.1 | convolution fusion | flops 21462784 | bytes 1017856 | tf_op jit(solution)/shard_map/while/body/eval_jaxpr/qd,kd->qk/dot_general | solution.py:47
  80.8 1.3 %fusion.54 = (f32[256]{0:T(256)S(1)}, f32[256,640]{1,0:T(8,128)S(1)}) fusion(pred[256,640]{1,0:T(32,128)(4,1)S(1)} %fusion.53, bf16[8,640,64]{2,1,0:T(8,128)(2,1)} %get-tuple-element.234, s32[]{:T(128)S(6)} %copy.62, bf16[8,256,64]{1,2,0:T(8,128)(2,1)} %get-tuple-element.233), kind=kOutput, calls=%fused_computation.76.clone.1 | convolution fusion | flops 21462784 | bytes 1017856 | tf_op jit(solution)/shard_map/while/body/eval_jaxpr/qd,kd->qk/dot_general | solution.py:47
  84.1 1.3 %fusion.54 = (f32[256]{0:T(256)S(1)}, f32[256,640]{1,0:T(8,128)S(1)}) fusion(pred[256,640]{1,0:T(32,128)(4,1)S(1)} %fusion.53, bf16[8,640,64]{2,1,0:T(8,128)(2,1)} %get-tuple-element.234, s32[]{:T(128)S(6)} %copy.62, bf16[8,256,64]{1,2,0:T(8,128)(2,1)} %get-tuple-element.233), kind=kOutput, calls=%fused_computation.76.clone.1 | convolution fusion | flops 21462784 | bytes 1017856 | tf_op jit(solution)/shard_map/while/body/eval_jaxpr/qd,kd->qk/dot_general | solution.py:47
  87.2 2.2 %all_gather.7 = bf16[256,1024]{0,1:T(8,128)(2,1)S(1)} all-gather(bf16[256,512]{0,1:T(8,128)(2,1)S(1)} %bitcast.72), channel_id=1, replica_groups=mesh['dp'=4,'kv'=4,'tp'=2] {'tp'}, dimensions={1}, use_global_device_ids=true | all-gather | bytes 786432 | tf_op jit(solution)/shard_map/all_gather | solution.py:139
  89.3 1.5 %convolution_convert_fusion = bf16[256,1024]{1,0:T(8,128)(2,1)} fusion(bf16[256,1024]{0,1:T(8,128)(2,1)S(1)} %all_gather.7, bf16[1024,1024]{1,0:T(8,128)(2,1)S(1)} %copy-done), kind=kOutput, calls=%fused_computation.29 | convolution fusion | flops 537133056 | bytes 3145728 | tf_op jit(solution)/shard_map/dot_general | solution.py:138
  (112 shorter events, 26.5 us)
Async XLA Ops:
  6.5 82.8 %copy-start = (bf16[1024,1024]{1,0:T(8,128)(2,1)S(1)}, bf16[1024,1024]{1,0:T(8,128)(2,1)}, u32[]{:S(2)}) copy-start(bf16[1024,1024]{1,0:T(8,128)(2,1)} %param.12) | copy-start | bytes 6291460
  6.5 14.9 %all-gather.2.cloned.1.call-start = ((), (), s32[]{:S(2)}) async-start(), calls=%async_computation.3 | async-start | bytes 1572864 | tf_op jit(solution)/shard_map/all_gather | solution.py:72
  9.3 11.8 %all-to-all-start = ((s32[4,1,3]{2,1,0:T(1,128)}), s32[4,1,3]{2,1,0:T(1,128)S(1)}, u32[]{:S(2)}, u32[]{:S(2)}) async-start(s32[4,1,3]{2,1,0:T(1,128)} %copy.41), calls=%async_computation | async-start | bytes 4096 | tf_op jit(solution)/shard_map/all_to_all | solution.py:105
  16.0 8.4 %copy-start.4 = (f32[256,32]{0,1:T(8,128)}, f32[256,32]{0,1:T(8,128)S(1)}, u32[]{:S(2)}) copy-start(f32[256,32]{0,1:T(8,128)S(1)} %get-tuple-element.133) | copy-start | bytes 98308
  16.0 8.4 %copy-start.5 = (f32[256,32]{0,1:T(8,128)}, f32[256,32]{0,1:T(8,128)S(1)}, u32[]{:S(2)}) copy-start(f32[256,32]{0,1:T(8,128)S(1)} %get-tuple-element.134) | copy-start | bytes 98308
  24.3 7.4 %copy-start.7 = (s32[8,16]{1,0:T(8,128)S(1)}, s32[8,16]{1,0:T(8,128)}, u32[]{:S(2)}) copy-start(s32[8,16]{1,0:T(8,128)} %param.13) | copy-start | bytes 1540
  26.4 16.2 %all-to-all-start.1 = ((bf16[4,3,32,512]{3,2,1,0:T(8,128)(2,1)}), bf16[4,3,32,512]{3,2,1,0:T(8,128)(2,1)S(1)}, u32[]{:S(2)}, u32[]{:S(2)}) async-start(bf16[4,3,32,512]{3,2,1,0:T(8,128)(2,1)} %bitcast.5), calls=%async_computation.1 | async-start | bytes 786432 | tf_op jit(solution)/shard_map/all_to_all | solution.py:109
  42.7 7.8 %copy-start.2 = (bf16[4,3,32,512]{3,2,1,0:T(8,128)(2,1)}, bf16[4,3,32,512]{3,2,1,0:T(8,128)(2,1)S(1)}, u32[]{:S(2)}) copy-start(bf16[4,3,32,512]{3,2,1,0:T(8,128)(2,1)S(1)} %all-to-all-done.1) | copy-start | bytes 1179652
  42.7 15.5 %all-to-all-start.2 = ((bf16[4,3,32,512]{3,2,1,0:T(8,128)(2,1)}), bf16[4,3,32,512]{3,2,1,0:T(8,128)(2,1)}, u32[]{:S(2)}, u32[]{:S(2)}) async-start(bf16[4,3,32,512]{3,2,1,0:T(8,128)(2,1)} %bitcast.9), calls=%async_computation.2 | async-start | bytes 786432 | tf_op jit(solution)/shard_map/all_to_all | solution.py:110
  55.3 4.4 %copy-start.1 = (bf16[256,8,64]{2,1,0:T(8,128)(2,1)S(1)}, bf16[256,8,64]{2,1,0:T(8,128)(2,1)}, u32[]{:S(2)}) copy-start(bf16[256,8,64]{2,1,0:T(8,128)(2,1)} %copy.46) | copy-start | bytes 786436
  59.7 1.6 %copy-start.6 = (pred[640]{0:T(1024)(128)(4,1)S(1)}, pred[640]{0:T(1024)(128)(4,1)}, u32[]{:S(2)}) copy-start(pred[640]{0:T(1024)(128)(4,1)} %concatenate.45) | copy-start | bytes 1924
  59.7 1.6 %copy-start.8 = (f32[8,256]{1,0:T(8,128)S(1)}, f32[8,256]{1,0:T(8,128)}, u32[]{:S(2)}) copy-start(f32[8,256]{1,0:T(8,128)} %custom-call.4) | copy-start | bytes 24580
  60.0 1.3 %copy-start.3 = (f32[8,256,64]{1,2,0:T(8,128)S(1)}, f32[8,256,64]{1,2,0:T(8,128)}, u32[]{:S(2)}) copy-start(f32[8,256,64]{1,2,0:T(8,128)} %custom-call.5) | copy-start | bytes 1572868
Sparse Core Ops, SparseCore 0:
  8.9 11.7 all-gather.1
where the time goes:
time: 98.5 us; the launch traced here: 97.7 us
  matrix products  31.3 us (32%)
  starting transfers between devices  14.6 us (15%)
  waiting for transfers between devices  14.3 us (15%)
  between operations  13.7 us (14%)
  local copies, waits for them, and re-layouts  13.3 us (14%)
  other arithmetic  8.01 us (8%)
  blocking collectives  2.18 us (2%)
    dot_general x8, matrix products, one_head(): jnp.einsum('qd,kd->qk', query_head, key_head, preferred_element_type=jnp....  10.5 us
    dot_general x8, matrix products, one_head(): jnp.dot(weights.astype(jnp.bfloat16), value_head, preferred_element_type=...  10.2 us
    dot_general x3, matrix products, on_device(): jnp.dot(fragment, weight, preferred_element_type=jnp.float32)  9.11 us
    all_to_all x1, waiting for transfers between devices, on_device(): lax.all_to_all(key_store[incoming], 'kv', split_axis=0, concat_axis=0, ti...  6.89 us
    all_to_all x1, starting transfers between devices, on_device(): lax.all_to_all(request, 'kv', split_axis=0, concat_axis=0, tiled=True)  6.35 us
    all_to_all x1, waiting for transfers between devices, on_device(): lax.all_to_all(request, 'kv', split_axis=0, concat_axis=0, tiled=True)  5.08 us
    all_to_all x1, starting transfers between devices, on_device(): lax.all_to_all(value_store[incoming], 'kv', split_axis=0, concat_axis=0,...  4.12 us
    all_to_all x1, starting transfers between devices, on_device(): lax.all_to_all(key_store[incoming], 'kv', split_axis=0, concat_axis=0, ti...  4.09 us
  transfers between devices with their start and end apart: 4, of which 3 were waited for; matrix products, arithmetic and copies ran while one was open for 18% of the time, Pallas kernels for 0%

commit v1 on v0

v1 whole, which is shorter than its diff:
```python
import functools

import jax
import jax.numpy as jnp
from jax import lax
from jax.experimental import pallas as pl
from jax.experimental.pallas import tpu as pltpu
from jax.sharding import PartitionSpec as P


HEAD_DIM = 64
BLOCK = 32
CAP = 3
LANES = 128

rotary_base = 500000.0
masked_score = -1e30
score_factor = HEAD_DIM ** (-0.5) * 1.4426950408889634


VMEM = pl.BlockSpec(memory_space=pltpu.VMEM)


def call(kernel, operands, results, flops=1000000, limit=16, scratch=(), far=0):
    anywhere = pl.BlockSpec(memory_space=pl.ANY)
    near = len(operands) - far
    out = pl.pallas_call(
        kernel,
        in_specs=[VMEM] * near + [anywhere] * far,
        out_specs=[anywhere if r.memory_space == pltpu.HBM else VMEM for r in results],
        out_shape=results,
        scratch_shapes=list(scratch),
        cost_estimate=pl.CostEstimate(flops=flops, bytes_accessed=100000, transcendentals=0),
        compiler_params=pltpu.CompilerParams(vmem_limit_bytes=limit << 20),
    )(
        *[pltpu.with_memory_space_constraint(x, pltpu.VMEM) for x in operands[:near]],
        *[pltpu.with_memory_space_constraint(x, pltpu.HBM) for x in operands[near:]],
    )
    return out[0] if len(results) == 1 else out


def dot(left, right):
    return jnp.dot(left, right, preferred_element_type=jnp.float32)


def table_kernel(angle_ref, cos_ref, sin_ref):
    blocks = cos_ref.shape[0] // BLOCK
    cosine, sine = jnp.cos(angle_ref[...]), jnp.sin(angle_ref[...])
    lane = lax.broadcasted_iota(jnp.int32, (BLOCK, LANES), 1)
    sign = jnp.where(lane % HEAD_DIM < HEAD_DIM // 2, -1.0, 1.0)
    cos_in, sin_in = cosine[:BLOCK], sine[:BLOCK]
    for block in range(blocks):
        rows = slice(block * BLOCK, (block + 1) * BLOCK)
        cos_at = cosine[BLOCK + block : BLOCK + block + 1]
        sin_at = sine[BLOCK + block : BLOCK + block + 1]
        cos_ref[rows, :] = cos_in * cos_at - sin_in * sin_at
        sin_ref[rows, :] = (sin_in * cos_at + cos_in * sin_at) * sign


def rotary_tables(first_pos, rows):
    half = HEAD_DIM // 2
    inverse = 1.0 / rotary_base ** (jnp.arange(half, dtype=jnp.float32) / half)
    inverse = jnp.tile(inverse, LANES // half)
    offsets = jnp.arange(BLOCK, dtype=jnp.int32)
    starts = first_pos + BLOCK * jnp.arange(rows // BLOCK, dtype=jnp.int32)
    positions = jnp.concatenate([offsets, starts]).astype(jnp.float32)
    table = pltpu.VMEM((rows, LANES), jnp.float32)
    return call(table_kernel, [positions[:, None] * inverse[None, :]], [table] * 2)


def rotate(acc, cosine, sine):
    half = HEAD_DIM // 2
    lane = lax.broadcasted_iota(jnp.int32, (acc.shape[0], LANES), 1)
    first = lane % HEAD_DIM < half
    partner = jnp.where(first, pltpu.roll(acc, LANES - half, 1), pltpu.roll(acc, half, 1))
    return acc * cosine + partner * sine


def half_rows(weight_ref, other):
    mine = lax.axis_index("tp")
    depth = weight_ref.shape[0] // 2
    half = 1 - mine if other else mine
    return pl.ds(pl.multiple_of(half * depth, depth), depth)


def key_value_own_kernel(
    tokens_ref, key_ref, value_ref, part_ref, own_ref, key_rest_ref, value_rest_ref, key_own_ref,
    value_own_ref, sems
):
    width = key_ref.shape[1]
    mine, rest = half_rows(key_ref, False), half_rows(key_ref, True)
    copies = [
        pltpu.make_async_copy(source, target, sems.at[i])
        for i, (source, target) in enumerate(
            [
                (tokens_ref, own_ref),
                (key_ref.at[mine, :], key_own_ref),
                (value_ref.at[mine, :], value_own_ref),
                (key_ref.at[rest, :], key_rest_ref),
                (value_ref.at[rest, :], value_rest_ref),
            ]
        )
    ]
    for copy in copies:
        copy.start()
    copies[0].wait()
    copies[1].wait()
    part_ref[:, :width] = dot(own_ref[...], key_own_ref[...])
    copies[2].wait()
    part_ref[:, width:] = dot(own_ref[...], value_own_ref[...])
    copies[3].wait()
    copies[4].wait()


def key_value_kernel(part_ref, other_ref, key_ref, value_ref, cos_ref, sin_ref, out_ref):
    width = key_ref.shape[1]
    key_acc = part_ref[:, :width] + dot(other_ref[...], key_ref[...])
    cosine, sine = cos_ref[...], sin_ref[...]
    for start in range(0, width, LANES):
        lanes = slice(start, start + LANES)
        out_ref[:, lanes] = rotate(key_acc[:, lanes], cosine, sine).astype(jnp.bfloat16)
    value_acc = part_ref[:, width:] + dot(other_ref[...], value_ref[...])
    out_ref[:, width:] = value_acc.astype(jnp.bfloat16)


def query_kernel(own_ref, other_ref, weight_ref, cos_ref, sin_ref, out_ref):
    acc = dot(own_ref[...], weight_ref[half_rows(weight_ref, False), :]) + dot(
        other_ref[...], weight_ref[half_rows(weight_ref, True), :]
    )
    cosine, sine = cos_ref[...], sin_ref[...]
    for start in range(0, acc.shape[1], LANES):
        lanes = slice(start, start + LANES)
        out_ref[:, lanes] = rotate(acc[:, lanes], cosine, sine).astype(jnp.bfloat16)


def pick_kernel(asked_ref, store_ref, out_ref):
    blocks = store_ref.shape[0] // BLOCK
    first = lax.axis_index("kv") * blocks
    asked = asked_ref[...]
    count = jnp.int32(0)
    index = [jnp.int32(0)] * CAP
    for block in range(blocks):
        hit = jnp.max((asked == first + block).astype(jnp.int32))
        for slot in range(CAP):
            index[slot] = jnp.where((hit == 1) & (count == slot), block, index[slot])
        count = count + hit
    for slot in range(CAP):
        rows = pl.ds(pl.multiple_of(index[slot] * BLOCK, BLOCK), BLOCK)
        out_ref[slot * BLOCK : (slot + 1) * BLOCK, :] = store_ref[rows, :]


def list_kernel(devices, chosen_ref, local_ref, remote_ref):
    blocks, slots = chosen_ref.shape
    rows = local_ref.shape[1]
    device = lax.axis_index("kv")
    spread = (
        lax.broadcasted_iota(jnp.int32, (blocks, rows), 1) // BLOCK
        == lax.broadcasted_iota(jnp.int32, (blocks, rows), 0)
    ).astype(jnp.float32)
    listed_ids = lax.dot_general(
        chosen_ref[...].astype(jnp.float32),
        spread,
        (((0,), (0,)), ((), ())),
        precision=lax.Precision.HIGHEST,
        preferred_element_type=jnp.float32,
    )
    row = lax.broadcasted_iota(jnp.int32, (blocks, rows), 0)
    for shift in range(devices):
        source = device - shift
        ids = jnp.where(source >= 0, source * blocks + row, -2).astype(jnp.float32)
        listed = jnp.zeros((blocks, rows), jnp.float32)
        for slot in range(slots):
            listed = jnp.where(listed_ids[slot : slot + 1, :] == ids, 1.0, listed)
        if shift == 0:
            local_ref[...] = jnp.where(listed > 0.0, 0.0, masked_score)
            continue
        needed = jnp.broadcast_to(jnp.max(listed, axis=1, keepdims=True), (blocks, rows))
        rank, step = needed, 1
        while step < blocks:
            rank = rank + jnp.where(row >= step, pltpu.roll(rank, step, 0), 0.0)
            step *= 2
        for slot in range(CAP):
            here = jnp.where((needed > 0.0) & (rank == slot + 1.0), listed, 0.0)
            hit = jnp.max(here, axis=0, keepdims=True)
            at = (shift - 1) * CAP + slot
            remote_ref[at : at + 1, :] = jnp.where(hit > 0.0, 0.0, masked_score)


def head_pair_queries(queries):
    lane = lax.broadcasted_iota(jnp.int32, queries.shape, 1)
    zero = jnp.zeros_like(queries)
    return jnp.concatenate(
        [jnp.where(lane < HEAD_DIM, queries, zero), jnp.where(lane < HEAD_DIM, zero, queries)],
        axis=0,
    )


def pair_scores(keys, queries):
    return lax.dot_general(
        keys, queries, (((1,), (1,)), ((), ())), preferred_element_type=jnp.float32
    )


def pair_values(values, weights):
    both = lax.dot_general(
        values, weights, (((0,), (0,)), ((), ())), preferred_element_type=jnp.float32
    )
    rows = weights.shape[1] // 2
    return jnp.concatenate([both[:HEAD_DIM, :rows], both[HEAD_DIM:, rows:]], axis=0)


def widen(stat):
    rows = stat.shape[1] // 2
    return jnp.concatenate(
        [
            jnp.broadcast_to(stat[:, :rows], (HEAD_DIM, rows)),
            jnp.broadcast_to(stat[:, rows:], (HEAD_DIM, rows)),
        ],
        axis=0,
    )


def local_kernel(query_ref, store_ref, bias_ref, peak_ref, total_ref, summed_ref):
    rows, width = query_ref.shape
    blocks = rows // BLOCK
    listed = jnp.concatenate(
        [jnp.broadcast_to(bias_ref[b : b + 1, :], (BLOCK, rows)) for b in range(blocks)], axis=0
    )
    key_row = lax.broadcasted_iota(jnp.int32, (rows, rows), 0)
    query_row = lax.broadcasted_iota(jnp.int32, (rows, rows), 1)
    bias = jnp.where(key_row <= query_row, listed, masked_score)
    bias = jnp.concatenate([bias, bias], axis=1)
    for pair in range(width // LANES):
        lanes = slice(pair * LANES, (pair + 1) * LANES)
        queries = head_pair_queries(query_ref[:, lanes])
        scores = pair_scores(store_ref[:, lanes], queries) + bias
        peak = jnp.max(scores, axis=0, keepdims=True)
        weights = jnp.exp2((scores - peak) * score_factor)
        peak_ref[pair : pair + 1, :] = peak
        total_ref[pair : pair + 1, :] = jnp.sum(weights, axis=0, keepdims=True)
        values = store_ref[:, width + pair * LANES : width + (pair + 1) * LANES]
        summed_ref[lanes, :] = pair_values(values, weights.astype(jnp.bfloat16))


def remote_kernel(shift, last, query_ref, bias_ref, got_ref, *refs):
    (peak_ref, total_ref, summed_ref), out_refs = refs[:3], refs[3:]
    rows, width = query_ref.shape
    first = (shift - 1) * CAP
    bias = jnp.concatenate(
        [jnp.broadcast_to(bias_ref[first + s : first + s + 1, :], (BLOCK, rows)) for s in range(CAP)],
        axis=0,
    )
    bias = jnp.concatenate([bias, bias], axis=1)
    for pair in range(width // LANES):
        lanes = slice(pair * LANES, (pair + 1) * LANES)
        queries = head_pair_queries(query_ref[:, lanes])
        peak = peak_ref[pair : pair + 1, :]
        scores = pair_scores(got_ref[:, lanes], queries) + bias
        peak_new = jnp.maximum(peak, jnp.max(scores, axis=0, keepdims=True))
        factor = jnp.exp2((peak - peak_new) * score_factor)
        weights = jnp.exp2((scores - peak_new) * score_factor)
        total = total_ref[pair : pair + 1, :] * factor + jnp.sum(weights, axis=0, keepdims=True)
        values = got_ref[:, width + pair * LANES : width + (pair + 1) * LANES]
        summed = summed_ref[lanes, :] * widen(factor) + pair_values(
            values, weights.astype(jnp.bfloat16)
        )
        if last:
            out_refs[0][:, lanes] = (summed / widen(total)).T.astype(jnp.bfloat16)
        else:
            out_refs[0][pair : pair + 1, :] = peak_new
            out_refs[1][pair : pair + 1, :] = total
            out_refs[2][lanes, :] = summed


def out_own_kernel(own_ref, weight_ref, out_ref):
    out_ref[...] = dot(own_ref[...], weight_ref[half_rows(weight_ref, False), :])


def out_kernel(part_ref, other_ref, weight_ref, out_ref, tile_ref, sems):
    tiles = tile_ref.shape[0]
    width = tile_ref.shape[2]
    rows = half_rows(weight_ref, True)
    copies = []
    for tile in range(tiles):
        lanes = slice(tile * width, (tile + 1) * width)
        acc = part_ref[:, lanes] + dot(other_ref[...], weight_ref[rows, lanes])
        tile_ref[tile] = acc.astype(jnp.bfloat16)
        copies.append(
            pltpu.make_async_copy(tile_ref.at[tile], out_ref.at[:, lanes], sems.at[tile])
        )
        copies[-1].start()
    for copy in copies:
        copy.wait()


def on_device(tokens, query_weight, key_weight, value_weight, out_weight, chosen):
    rows, depth = tokens.shape
    width = query_weight.shape[1]
    pairs = width // LANES
    device = lax.axis_index("kv")
    devices = lax.axis_size("kv")
    swap = [(0, 1), (1, 0)]

    def turn(x, by):
        return lax.ppermute(x, "kv", [(i, (i + by) % devices) for i in range(devices)])

    other = lax.ppermute(tokens, "tp", swap)
    asked = []
    for shift in range(1, devices):
        asked.append(turn(chosen, -shift))
    cosine, sine = rotary_tables(device * rows, rows)
    half = pltpu.VMEM((depth, width), jnp.bfloat16)
    part, own, key_rest, value_rest = call(
        key_value_own_kernel,
        [tokens, key_weight, value_weight],
        [
            pltpu.VMEM((rows, 2 * width), jnp.float32),
            pltpu.VMEM((rows, depth), jnp.bfloat16),
            half,
            half,
        ],
        flops=4 * rows * depth * width,
        scratch=[half, half, pltpu.SemaphoreType.DMA((5,))],
        far=3,
    )
    store = call(
        key_value_kernel,
        [part, other, key_rest, value_rest, cosine, sine],
        [pltpu.VMEM((rows, 2 * width), jnp.bfloat16)],
        flops=4 * rows * depth * width,
    )
    got = []
    for shift in range(1, devices):
        picked = call(
            pick_kernel,
            [asked[shift - 1], store],
            [pltpu.VMEM((CAP * BLOCK, 2 * width), jnp.bfloat16)],
        )
        got.append(turn(picked, shift))
    queries = call(
        query_kernel,
        [own, other, query_weight, cosine, sine],
        [pltpu.VMEM((rows, width), jnp.bfloat16)],
        flops=4 * rows * depth * width,
    )
    remote_rows = max(8, (devices - 1) * CAP)
    local_bias, remote_bias = call(
        functools.partial(list_kernel, devices),
        [chosen],
        [
            pltpu.VMEM((rows // BLOCK, rows), jnp.float32),
            pltpu.VMEM((remote_rows, rows), jnp.float32),
        ],
    )
    state_shapes = [
        pltpu.VMEM((pairs, 2 * rows), jnp.float32),
        pltpu.VMEM((pairs, 2 * rows), jnp.float32),
        pltpu.VMEM((width, rows), jnp.float32),
    ]
    attended_shape = [pltpu.VMEM((rows, width), jnp.bfloat16)]
    state = call(
        local_kernel, [queries, store, local_bias], state_shapes, flops=16 * rows * rows * width
    )
    for shift in range(1, devices):
        last = shift == devices - 1
        state = call(
            functools.partial(remote_kernel, shift, last),
            [queries, remote_bias, got[shift - 1], *state],
            attended_shape if last else state_shapes,
            flops=16 * rows * CAP * BLOCK * width,
        )
    attended = state
    attended_other = lax.ppermute(attended, "tp", swap)
    out_width = out_weight.shape[1]
    out_part = call(
        out_own_kernel,
        [attended, out_weight],
        [pltpu.VMEM((rows, out_width), jnp.float32)],
        flops=2 * rows * width * out_width,
    )
    tiles = 4
    return call(
        out_kernel,
        [out_part, attended_other, out_weight],
        [pltpu.HBM((rows, out_width), jnp.bfloat16)],
        flops=2 * rows * width * out_width,
        scratch=[
            pltpu.VMEM((tiles, rows, out_width // tiles), jnp.bfloat16),
            pltpu.SemaphoreType.DMA((tiles,)),
        ],
    )


def solution(mesh):
    placed = (
        P(("dp", "kv"), "tp"),
        P(None, "tp"),
        P(None, "tp"),
        P(None, "tp"),
        P(None, "tp"),
        P(("dp", "kv"), None),
    )
    return jax.shard_map(
        on_device, mesh=mesh, in_specs=placed, out_specs=P(("dp", "kv"), "tp"), check_vma=False
    )
```

time: 98.5 us -> 40 us (0.41)
  matrix products: 31.3 us -> 0 us
  between operations: 13.7 us -> 0.2 us
  local copies, waits for them, and re-layouts: 13.3 us -> 0.11 us
  Pallas kernels: 0 us -> 12 us
  other arithmetic: 8.01 us -> 0.17 us
  blocking collectives: 2.18 us -> 0 us
  starting transfers between devices: 14.6 us -> 12.6 us
    dot_general x20 -> x0, matrix products: 31.3 us -> none  [the longest x8 10.5 us: one_head(): jnp.einsum('qd,kd->qk', query_head, key_head, preferred_element_type=jnp....]
    ppermute x0 -> x8, waiting for transfers between devices: none -> 14.9 us  [the longest x6 13.8 us: turn(): lax.ppermute(x, 'kv', [(i, (i + by) % devices) for i in range(devices)])]
    all_to_all x3 -> x0, starting transfers between devices: 14.6 us -> none  [the longest x1 6.35 us: on_device(): lax.all_to_all(request, 'kv', split_axis=0, concat_axis=0, tiled=True)]
    all_to_all x3 -> x0, waiting for transfers between devices: 13.5 us -> none  [the longest x1 6.89 us: on_device(): lax.all_to_all(key_store[incoming], 'kv', split_axis=0, concat_axis=0, ti...]
    ppermute x0 -> x8, starting transfers between devices: none -> 12.6 us  [the longest x6 12 us: turn(): lax.ppermute(x, 'kv', [(i, (i + by) % devices) for i in range(devices)])]
    pallas_call x0 -> x14, Pallas kernels: none -> 12 us  [call(): pl.pallas_call(kernel, in_specs=[VMEM] * near + [anywhere] * far, out_spe...]
    concatenate x4 -> x0, local copies, waits for them, and re-layouts: 4.73 us -> none  [the longest x2 2.61 us: on_device(): jnp.concatenate([value_proj, got_values.reshape(-1, head_width)], axis=0)]
    reduce_sum x9 -> x0, other arithmetic: 3.04 us -> none  [the longest x8 2.89 us: one_head(): denominator = denominator * factor + jnp.sum(weights, axis=1)]
  transfers between devices with their start and end apart: 4 -> 8, of which waited for: 3 -> 4; matrix products, arithmetic and copies ran while one was open for 18% -> 1% of each run, Pallas kernels for 0% -> 23%
where the time goes in v1:
time: 40 us; the launch traced here: 39.9 us
  waiting for transfers between devices  14.9 us (37%)
  starting transfers between devices  12.6 us (32%)
  Pallas kernels  12 us (30%)
    ppermute x6, waiting for transfers between devices, turn(): lax.ppermute(x, 'kv', [(i, (i + by) % devices) for i in range(devices)])  13.8 us
    ppermute x6, starting transfers between devices, turn(): lax.ppermute(x, 'kv', [(i, (i + by) % devices) for i in range(devices)])  12 us
    pallas_call x14, Pallas kernels, call(): pl.pallas_call(kernel, in_specs=[VMEM] * near + [anywhere] * far, out_spe...  12 us
    ppermute x1, waiting for transfers between devices, on_device(): attended_other = lax.ppermute(attended, 'tp', swap)  1.06 us
  transfers between devices with their start and end apart: 8, of which 4 were waited for; matrix products, arithmetic and copies ran while one was open for 1% of the time, Pallas kernels for 23%

profile of v1, /device:TPU:0, one launch (start us, length us, event | category | flops | bytes accessed | tf_op | source)
XLA Modules:
  0.0 39.9 jit_solution(6315422019090808514)
XLA Ops:
  0.0 0.5 %collective-permute-start = (bf16[256,1024]{1,0:T(8,128)(2,1)}, bf16[256,1024]{1,0:T(8,128)(2,1)S(1)}, u32[]{:S(2)}, u32[]{:S(2)}) collective-permute-start(bf16[256,1024]{1,0:T(8,128)(2,1)} %tokens_ref.1), channel_id=1, source_target_pairs={{0,1},{1,0},{2,3},{3,2},{4,5},{5,4},{6,7},{7,6},{8,9},{9,8},{10,11... | collective-permute-start | bytes 1572872 | tf_op jit(solution)/shard_map/ppermute | solution.py:307
  0.5 4.6 %collective-permute-start.5 = (s32[8,16]{1,0:T(8,128)}, s32[8,16]{1,0:T(8,128)S(1)}, u32[]{:S(2)}, u32[]{:S(2)}) collective-permute-start(s32[8,16]{1,0:T(8,128)} %chosen_ref.1), channel_id=1, source_target_pairs={{0,6},{2,0},{4,2},{6,4},{1,7},{3,1},{5,3},{7,5},{8,14},{10,8},{12,... | collective-permute-start | bytes 1544 | tf_op jit(solution)/shard_map/ppermute | solution.py:305
  5.1 0.1 mul.26
  5.3 0.1 shard_map.65
  5.5 2.4 %shard_map.64 = (f32[256,1024]{1,0:T(8,128)S(1)}, bf16[256,1024]{1,0:T(8,128)(2,1)S(1)}, bf16[1024,512]{1,0:T(8,128)(2,1)S(1)}, bf16[1024,512]{1,0:T(8,128)(2,1)S(1)}) custom-call(bf16[256,1024]{1,0:T(8,128)(2,1)} %tokens_ref.1, bf16[2048,512]{1,0:T(8,128)(2,1)} %key_ref.1, bf16[2048,512]{1,0:T(8,128)(2,1)} %value_ref.1), custom_call_target="tpu_custom_call" | custom-call | flops 536870912 | bytes 100000 | tf_op jit(solution)/shard_map/pallas_call | solution.py:27
  7.9 0.7 %shard_map.68.store_ref = bf16[256,1024]{1,0:T(8,128)(2,1)S(1)} custom-call(f32[256,1024]{1,0:T(8,128)S(1)} %get-tuple-element.26.part_ref, bf16[256,1024]{1,0:T(8,128)(2,1)S(1)} %collective-permute-done.other_ref, bf16[1024,512]{1,0:T(8,128)(2,1)S(1)} %get-tuple-element.27.key_ref, bf16[1024,512]{1,0:T(8,128)(2,1)S(1)} %get-tuple-element.28.value_ref, ...), custom_call_target="tpu_custom_call" | custom-call | flops 536870912 | bytes 100000 | tf_op jit(solution)/shard_map/pallas_call | solution.py:27
  8.6 0.2 shard_map.71
  9.0 2.6 %collective-permute-start.3 = (s32[8,16]{1,0:T(8,128)S(1)}, s32[8,16]{1,0:T(8,128)S(1)}, u32[]{:S(2)}, u32[]{:S(2)}) collective-permute-start(s32[8,16]{1,0:T(8,128)S(1)} %copy-done.2), channel_id=1, source_target_pairs={{0,4},{2,6},{4,0},{6,2},{1,5},{3,7},{5,1},{7,3},{8,12},{10,14},{12... | collective-permute-start | bytes 1544 | tf_op jit(solution)/shard_map/ppermute | solution.py:305
  11.6 2.3 %collective-permute-done.3.asked_ref = s32[8,16]{1,0:T(8,128)S(1)} collective-permute-done((s32[8,16]{1,0:T(8,128)S(1)}, s32[8,16]{1,0:T(8,128)S(1)}, u32[]{:S(2)}, u32[]{:S(2)}) %collective-permute-start.3) | collective-permute-done | bytes 544 | tf_op jit(solution)/shard_map/ppermute | solution.py:305
  13.9 0.2 shard_map.70
  14.1 3.4 %collective-permute-start.4 = (bf16[96,1024]{1,0:T(8,128)(2,1)S(1)}, bf16[96,1024]{1,0:T(8,128)(2,1)S(1)}, u32[]{:S(2)}, u32[]{:S(2)}) collective-permute-start(bf16[96,1024]{1,0:T(8,128)(2,1)S(1)} %shard_map.70), channel_id=1, source_target_pairs={{0,4},{2,6},{4,0},{6,2},{1,5},{3,7},{5,1},{7,3},{8,12},{10,14},{12... | collective-permute-start | bytes 589832 | tf_op jit(solution)/shard_map/ppermute | solution.py:305
  17.6 1.2 %collective-permute-start.1 = (s32[8,16]{1,0:T(8,128)S(1)}, s32[8,16]{1,0:T(8,128)S(1)}, u32[]{:S(2)}, u32[]{:S(2)}) collective-permute-start(s32[8,16]{1,0:T(8,128)S(1)} %copy-done.2), channel_id=1, source_target_pairs={{0,2},{2,4},{4,6},{6,0},{1,3},{3,5},{5,7},{7,1},{8,10},{10,12},{12... | collective-permute-start | bytes 1544 | tf_op jit(solution)/shard_map/ppermute | solution.py:305
  18.8 6.3 %collective-permute-done.1.asked_ref = s32[8,16]{1,0:T(8,128)S(1)} collective-permute-done((s32[8,16]{1,0:T(8,128)S(1)}, s32[8,16]{1,0:T(8,128)S(1)}, u32[]{:S(2)}, u32[]{:S(2)}) %collective-permute-start.1) | collective-permute-done | bytes 544 | tf_op jit(solution)/shard_map/ppermute | solution.py:305
  25.1 0.2 shard_map.69
  25.4 0.3 shard_map.67
  25.8 1.0 %shard_map.66.query_ref = bf16[256,512]{1,0:T(8,128)(2,1)S(1)} custom-call(bf16[256,1024]{1,0:T(8,128)(2,1)S(1)} %get-tuple-element.22.own_ref, bf16[256,1024]{1,0:T(8,128)(2,1)S(1)} %collective-permute-done.other_ref, bf16[2048,512]{1,0:T(8,128)(2,1)S(1)} %copy-done.1, f32[256,128]{1,0:T(8,128)S(1)} %get-tuple-element.23.cos_ref, ...), custom_call_target="tpu_custom_call" | custom-call | flops 536870912 | bytes 100000 | tf_op jit(solution)/shard_map/pallas_call | solution.py:27
  26.8 1.6 %shard_map.72 = (f32[4,512]{1,0:T(4,128)S(1)}, f32[4,512]{1,0:T(4,128)S(1)}, f32[512,256]{1,0:T(8,128)S(1)}) custom-call(bf16[256,512]{1,0:T(8,128)(2,1)S(1)} %shard_map.66.query_ref, bf16[256,1024]{1,0:T(8,128)(2,1)S(1)} %shard_map.68.store_ref, f32[8,256]{1,0:T(8,128)S(1)} %get-tuple-element.29.bias_ref), custom_call_target="tpu_custom_call" | custom-call | flops 536870912 | bytes 100000 | tf_op jit(solution)/shard_map/pallas_call | solution.py:27
  28.4 1.1 %shard_map.73 = (f32[4,512]{1,0:T(4,128)S(1)}, f32[4,512]{1,0:T(4,128)S(1)}, f32[512,256]{1,0:T(8,128)S(1)}) custom-call(bf16[256,512]{1,0:T(8,128)(2,1)S(1)} %shard_map.66.query_ref, f32[9,256]{1,0:T(8,128)S(1)} %get-tuple-element.25.bias_ref, bf16[96,1024]{1,0:T(8,128)(2,1)S(1)} %collective-permute-done.6.got_ref, f32[4,512]{1,0:T(4,128)S(1)} %get-tuple-element.30.refs_0_, ...), custom_call_target="tpu_custom_call" | custom-call | flops 201326592 | bytes 100000 | tf_op jit(solution)/shard_map/pallas_call | solution.py:27
  29.6 1.2 %shard_map.74 = (f32[4,512]{1,0:T(4,128)S(1)}, f32[4,512]{1,0:T(4,128)S(1)}, f32[512,256]{1,0:T(8,128)S(1)}) custom-call(bf16[256,512]{1,0:T(8,128)(2,1)S(1)} %shard_map.66.query_ref, f32[9,256]{1,0:T(8,128)S(1)} %get-tuple-element.25.bias_ref, bf16[96,1024]{1,0:T(8,128)(2,1)S(1)} %collective-permute-done.4.got_ref, f32[4,512]{1,0:T(4,128)S(1)} %get-tuple-element.33.refs_0_, ...), custom_call_target="tpu_custom_call" | custom-call | flops 201326592 | bytes 100000 | tf_op jit(solution)/shard_map/pallas_call | solution.py:27
  30.7 5.2 %collective-permute-done.2.got_ref = bf16[96,1024]{1,0:T(8,128)(2,1)S(1)} collective-permute-done((bf16[96,1024]{1,0:T(8,128)(2,1)S(1)}, bf16[96,1024]{1,0:T(8,128)(2,1)S(1)}, u32[]{:S(2)}, u32[]{:S(2)}) %collective-permute-start.2) | collective-permute-done | bytes 196640 | tf_op jit(solution)/shard_map/ppermute | solution.py:305
  35.9 1.2 %shard_map.75.own_ref = bf16[256,512]{1,0:T(8,128)(2,1)S(1)} custom-call(bf16[256,512]{1,0:T(8,128)(2,1)S(1)} %shard_map.66.query_ref, f32[9,256]{1,0:T(8,128)S(1)} %get-tuple-element.25.bias_ref, bf16[96,1024]{1,0:T(8,128)(2,1)S(1)} %collective-permute-done.2.got_ref, f32[4,512]{1,0:T(4,128)S(1)} %get-tuple-element.36.refs_0_, ...), custom_call_target="tpu_custom_call" | custom-call | flops 201326592 | bytes 100000 | tf_op jit(solution)/shard_map/pallas_call | solution.py:27
  37.2 0.4 %shard_map.76.part_ref = f32[256,1024]{1,0:T(8,128)S(1)} custom-call(bf16[256,512]{1,0:T(8,128)(2,1)S(1)} %shard_map.75.own_ref, bf16[1024,1024]{1,0:T(8,128)(2,1)S(1)} %copy-done), custom_call_target="tpu_custom_call" | custom-call | flops 268435456 | bytes 100000 | tf_op jit(solution)/shard_map/pallas_call | solution.py:27
  37.6 1.1 %collective-permute-done.7.other_ref = bf16[256,512]{1,0:T(8,128)(2,1)S(1)} collective-permute-done((bf16[256,512]{1,0:T(8,128)(2,1)S(1)}, bf16[256,512]{1,0:T(8,128)(2,1)S(1)}, u32[]{:S(2)}, u32[]{:S(2)}) %collective-permute-start.7) | collective-permute-done | bytes 262176 | tf_op jit(solution)/shard_map/ppermute | solution.py:373
  38.7 1.2 %shard_map.77 = bf16[256,1024]{1,0:T(8,128)(2,1)} custom-call(f32[256,1024]{1,0:T(8,128)S(1)} %shard_map.76.part_ref, bf16[256,512]{1,0:T(8,128)(2,1)S(1)} %collective-permute-done.7.other_ref, bf16[1024,1024]{1,0:T(8,128)(2,1)S(1)} %copy-done), custom_call_target="tpu_custom_call" | custom-call | flops 268435456 | bytes 100000 | tf_op jit(solution)/shard_map/pallas_call | solution.py:27
  (19 shorter events, 0.4 us)
Async XLA Ops:
  0.0 7.9 %collective-permute-start = (bf16[256,1024]{1,0:T(8,128)(2,1)}, bf16[256,1024]{1,0:T(8,128)(2,1)S(1)}, u32[]{:S(2)}, u32[]{:S(2)}) collective-permute-start(bf16[256,1024]{1,0:T(8,128)(2,1)} %tokens_ref.1), channel_id=1, source_target_pairs={{0,1},{1,0},{2,3},{3,2},{4,5},{5,4},{6,7},{7,6},{8,9},{9,8},{10,11... | collective-permute-start | bytes 1572872 | tf_op jit(solution)/shard_map/ppermute | solution.py:307
  0.5 8.1 %collective-permute-start.5 = (s32[8,16]{1,0:T(8,128)}, s32[8,16]{1,0:T(8,128)S(1)}, u32[]{:S(2)}, u32[]{:S(2)}) collective-permute-start(s32[8,16]{1,0:T(8,128)} %chosen_ref.1), channel_id=1, source_target_pairs={{0,6},{2,0},{4,2},{6,4},{1,7},{3,1},{5,3},{7,5},{8,14},{10,8},{12,... | collective-permute-start | bytes 1544 | tf_op jit(solution)/shard_map/ppermute | solution.py:305
  7.9 1.1 %copy-start.2 = (s32[8,16]{1,0:T(8,128)S(1)}, s32[8,16]{1,0:T(8,128)}, u32[]{:S(2)}) copy-start(s32[8,16]{1,0:T(8,128)} %chosen_ref.1) | copy-start | bytes 1540
  8.6 17.2 %copy-start.1 = (bf16[2048,512]{1,0:T(8,128)(2,1)S(1)}, bf16[2048,512]{1,0:T(8,128)(2,1)}, u32[]{:S(2)}) copy-start(bf16[2048,512]{1,0:T(8,128)(2,1)} %weight_ref.3) | copy-start | bytes 6291460
  8.9 19.5 %collective-permute-start.6 = (bf16[96,1024]{1,0:T(8,128)(2,1)S(1)}, bf16[96,1024]{1,0:T(8,128)(2,1)S(1)}, u32[]{:S(2)}, u32[]{:S(2)}) collective-permute-start(bf16[96,1024]{1,0:T(8,128)(2,1)S(1)} %shard_map.71), channel_id=1, source_target_pairs={{0,2},{2,4},{4,6},{6,0},{1,3},{3,5},{5,7},{7,1},{8,10},{10,12},{12... | collective-permute-start | bytes 589832 | tf_op jit(solution)/shard_map/ppermute | solution.py:305
  9.0 4.9 %collective-permute-start.3 = (s32[8,16]{1,0:T(8,128)S(1)}, s32[8,16]{1,0:T(8,128)S(1)}, u32[]{:S(2)}, u32[]{:S(2)}) collective-permute-start(s32[8,16]{1,0:T(8,128)S(1)} %copy-done.2), channel_id=1, source_target_pairs={{0,4},{2,6},{4,0},{6,2},{1,5},{3,7},{5,1},{7,3},{8,12},{10,14},{12... | collective-permute-start | bytes 1544 | tf_op jit(solution)/shard_map/ppermute | solution.py:305
  14.1 15.5 %collective-permute-start.4 = (bf16[96,1024]{1,0:T(8,128)(2,1)S(1)}, bf16[96,1024]{1,0:T(8,128)(2,1)S(1)}, u32[]{:S(2)}, u32[]{:S(2)}) collective-permute-start(bf16[96,1024]{1,0:T(8,128)(2,1)S(1)} %shard_map.70), channel_id=1, source_target_pairs={{0,4},{2,6},{4,0},{6,2},{1,5},{3,7},{5,1},{7,3},{8,12},{10,14},{12... | collective-permute-start | bytes 589832 | tf_op jit(solution)/shard_map/ppermute | solution.py:305
  17.6 7.6 %collective-permute-start.1 = (s32[8,16]{1,0:T(8,128)S(1)}, s32[8,16]{1,0:T(8,128)S(1)}, u32[]{:S(2)}, u32[]{:S(2)}) collective-permute-start(s32[8,16]{1,0:T(8,128)S(1)} %copy-done.2), channel_id=1, source_target_pairs={{0,2},{2,4},{4,6},{6,0},{1,3},{3,5},{5,7},{7,1},{8,10},{10,12},{12... | collective-permute-start | bytes 1544 | tf_op jit(solution)/shard_map/ppermute | solution.py:305
  25.4 10.5 %collective-permute-start.2 = (bf16[96,1024]{1,0:T(8,128)(2,1)S(1)}, bf16[96,1024]{1,0:T(8,128)(2,1)S(1)}, u32[]{:S(2)}, u32[]{:S(2)}) collective-permute-start(bf16[96,1024]{1,0:T(8,128)(2,1)S(1)} %shard_map.69), channel_id=1, source_target_pairs={{0,6},{2,0},{4,2},{6,4},{1,7},{3,1},{5,3},{7,5},{8,14},{10,8},{12,... | collective-permute-start | bytes 589832 | tf_op jit(solution)/shard_map/ppermute | solution.py:305
  28.4 8.8 %copy-start = (bf16[1024,1024]{1,0:T(8,128)(2,1)S(1)}, bf16[1024,1024]{1,0:T(8,128)(2,1)}, u32[]{:S(2)}) copy-start(bf16[1024,1024]{1,0:T(8,128)(2,1)} %weight_ref.5) | copy-start | bytes 6291460
  37.1 1.6 %collective-permute-start.7 = (bf16[256,512]{1,0:T(8,128)(2,1)S(1)}, bf16[256,512]{1,0:T(8,128)(2,1)S(1)}, u32[]{:S(2)}, u32[]{:S(2)}) collective-permute-start(bf16[256,512]{1,0:T(8,128)(2,1)S(1)} %shard_map.75.own_ref), channel_id=1, source_target_pairs={{0,1},{1,0},{2,3},{3,2},{4,5},{5,4},{6,7},{7,6},{8,9},{9,8},{10,11... | collective-permute-start | bytes 786440 | tf_op jit(solution)/shard_map/ppermute | solution.py:373

commit v2 on v1

--- a/solution.py
+++ b/solution.py
@@ -19,6 +19,16 @@
 
 
 VMEM = pl.BlockSpec(memory_space=pltpu.VMEM)
+
+
+def source_of(device, turn, devices):
+    if devices & (devices - 1) == 0:
+        return device ^ turn
+    return (device + devices - turn) % devices
+
+
+def turn_order(devices):
+    return [*range(2, devices), 1] if devices > 1 else []
 
 
 def call(kernel, operands, results, flops=1000000, limit=16, scratch=(), far=0):
@@ -43,29 +53,32 @@
     return jnp.dot(left, right, preferred_element_type=jnp.float32)
 
 
-def table_kernel(angle_ref, cos_ref, sin_ref):
-    blocks = cos_ref.shape[0] // BLOCK
-    cosine, sine = jnp.cos(angle_ref[...]), jnp.sin(angle_ref[...])
-    lane = lax.broadcasted_iota(jnp.int32, (BLOCK, LANES), 1)
-    sign = jnp.where(lane % HEAD_DIM < HEAD_DIM // 2, -1.0, 1.0)
-    cos_in, sin_in = cosine[:BLOCK], sine[:BLOCK]
-    for block in range(blocks):
-        rows = slice(block * BLOCK, (block + 1) * BLOCK)
-        cos_at = cosine[BLOCK + block : BLOCK + block + 1]
-        sin_at = sine[BLOCK + block : BLOCK + block + 1]
-        cos_ref[rows, :] = cos_in * cos_at - sin_in * sin_at
-        sin_ref[rows, :] = (sin_in * cos_at + cos_in * sin_at) * sign
-
-
-def rotary_tables(first_pos, rows):
+def table_kernel(cos_ref, sin_ref):
+    rows = cos_ref.shape[0]
     half = HEAD_DIM // 2
-    inverse = 1.0 / rotary_base ** (jnp.arange(half, dtype=jnp.float32) / half)
-    inverse = jnp.tile(inverse, LANES // half)
-    offsets = jnp.arange(BLOCK, dtype=jnp.int32)
-    starts = first_pos + BLOCK * jnp.arange(rows // BLOCK, dtype=jnp.int32)
-    positions = jnp.concatenate([offsets, starts]).astype(jnp.float32)
+    lane = lax.broadcasted_iota(jnp.int32, (BLOCK, LANES), 1) % half
+    inverse = jnp.zeros((BLOCK, LANES), jnp.float32)
+    for j in range(half):
+        inverse = jnp.where(lane == j, float(1.0 / rotary_base ** (j / half)), inverse)
+    offset = lax.broadcasted_iota(jnp.int32, (BLOCK, LANES), 0)
+    start = lax.axis_index("kv") * rows + BLOCK * offset
+    sign = jnp.where(
+        lax.broadcasted_iota(jnp.int32, (BLOCK, LANES), 1) % HEAD_DIM < half, -1.0, 1.0
+    )
+    angle_in = offset.astype(jnp.float32) * inverse
+    cos_in, sin_in = jnp.cos(angle_in), jnp.sin(angle_in)
+    angle_at = start.astype(jnp.float32) * inverse
+    cos_at, sin_at = jnp.cos(angle_at), jnp.sin(angle_at)
+    for block in range(rows // BLOCK):
+        at = slice(block * BLOCK, (block + 1) * BLOCK)
+        cos_b, sin_b = cos_at[block : block + 1], sin_at[block : block + 1]
+        cos_ref[at, :] = cos_in * cos_b - sin_in * sin_b
+        sin_ref[at, :] = (sin_in * cos_b + cos_in * sin_b) * sign
+
+
+def rotary_tables(rows):
     table = pltpu.VMEM((rows, LANES), jnp.float32)
-    return call(table_kernel, [positions[:, None] * inverse[None, :]], [table] * 2)
+    return call(table_kernel, [], [table] * 2, flops=2000000000)
 
 
 def rotate(acc, cosine, sine):
@@ -83,43 +96,22 @@
     return pl.ds(pl.multiple_of(half * depth, depth), depth)
 
 
-def key_value_own_kernel(
-    tokens_ref, key_ref, value_ref, part_ref, own_ref, key_rest_ref, value_rest_ref, key_own_ref,
-    value_own_ref, sems
-):
+def key_value_own_kernel(own_ref, key_ref, value_ref, out_ref):
     width = key_ref.shape[1]
-    mine, rest = half_rows(key_ref, False), half_rows(key_ref, True)
-    copies = [
-        pltpu.make_async_copy(source, target, sems.at[i])
-        for i, (source, target) in enumerate(
-            [
-                (tokens_ref, own_ref),
-                (key_ref.at[mine, :], key_own_ref),
-                (value_ref.at[mine, :], value_own_ref),
-                (key_ref.at[rest, :], key_rest_ref),
-                (value_ref.at[rest, :], value_rest_ref),
-            ]
-        )
-    ]
-    for copy in copies:
-        copy.start()
-    copies[0].wait()
-    copies[1].wait()
-    part_ref[:, :width] = dot(own_ref[...], key_own_ref[...])
-    copies[2].wait()
-    part_ref[:, width:] = dot(own_ref[...], value_own_ref[...])
-    copies[3].wait()
-    copies[4].wait()
+    rows = half_rows(key_ref, False)
+    out_ref[:, :width] = dot(own_ref[...], key_ref[rows, :])
+    out_ref[:, width:] = dot(own_ref[...], value_ref[rows, :])
 
 
 def key_value_kernel(part_ref, other_ref, key_ref, value_ref, cos_ref, sin_ref, out_ref):
     width = key_ref.shape[1]
-    key_acc = part_ref[:, :width] + dot(other_ref[...], key_ref[...])
+    rows = half_rows(key_ref, True)
+    key_acc = part_ref[:, :width] + dot(other_ref[...], key_ref[rows, :])
     cosine, sine = cos_ref[...], sin_ref[...]
     for start in range(0, width, LANES):
         lanes = slice(start, start + LANES)
         out_ref[:, lanes] = rotate(key_acc[:, lanes], cosine, sine).astype(jnp.bfloat16)
-    value_acc = part_ref[:, width:] + dot(other_ref[...], value_ref[...])
+    value_acc = part_ref[:, width:] + dot(other_ref[...], value_ref[rows, :])
     out_ref[:, width:] = value_acc.astype(jnp.bfloat16)
 
 
@@ -149,7 +141,10 @@
         out_ref[slot * BLOCK : (slot + 1) * BLOCK, :] = store_ref[rows, :]
 
 
-def list_kernel(devices, chosen_ref, local_ref, remote_ref):
+def list_kernel(devices, turns, far_ref, local_ref, remote_ref, chosen_ref, sem):
+    copy = pltpu.make_async_copy(far_ref, chosen_ref, sem)
+    copy.start()
+    copy.wait()
     blocks, slots = chosen_ref.shape
     rows = local_ref.shape[1]
     device = lax.axis_index("kv")
@@ -165,13 +160,13 @@
         preferred_element_type=jnp.float32,
     )
     row = lax.broadcasted_iota(jnp.int32, (blocks, rows), 0)
-    for shift in range(devices):
-        source = device - shift
-        ids = jnp.where(source >= 0, source * blocks + row, -2).astype(jnp.float32)
+    for place, turn in enumerate([0, *turns]):
+        source = source_of(device, turn, devices)
+        ids = jnp.where(source <= device, source * blocks + row, -2).astype(jnp.float32)
         listed = jnp.zeros((blocks, rows), jnp.float32)
         for slot in range(slots):
             listed = jnp.where(listed_ids[slot : slot + 1, :] == ids, 1.0, listed)
-        if shift == 0:
+        if turn == 0:
             local_ref[...] = jnp.where(listed > 0.0, 0.0, masked_score)
             continue
         needed = jnp.broadcast_to(jnp.max(listed, axis=1, keepdims=True), (blocks, rows))
@@ -182,7 +177,7 @@
         for slot in range(CAP):
             here = jnp.where((needed > 0.0) & (rank == slot + 1.0), listed, 0.0)
             hit = jnp.max(here, axis=0, keepdims=True)
-            at = (shift - 1) * CAP + slot
+            at = (place - 1) * CAP + slot
             remote_ref[at : at + 1, :] = jnp.where(hit > 0.0, 0.0, masked_score)
 
 
@@ -242,34 +237,45 @@
         summed_ref[lanes, :] = pair_values(values, weights.astype(jnp.bfloat16))
 
 
-def remote_kernel(shift, last, query_ref, bias_ref, got_ref, *refs):
-    (peak_ref, total_ref, summed_ref), out_refs = refs[:3], refs[3:]
+def remote_kernel(first, parts, last, query_ref, bias_ref, *refs):
+    got_refs, (peak_ref, total_ref, summed_ref) = refs[:parts], refs[parts : parts + 3]
+    out_refs = refs[parts + 3 :]
     rows, width = query_ref.shape
-    first = (shift - 1) * CAP
+    pairs = [slice(p * LANES, (p + 1) * LANES) for p in range(width // LANES)]
+    spans = [slice(width + p.start, width + p.stop) for p in pairs]
+    slots = range(first * CAP, (first + parts) * CAP)
     bias = jnp.concatenate(
-        [jnp.broadcast_to(bias_ref[first + s : first + s + 1, :], (BLOCK, rows)) for s in range(CAP)],
-        axis=0,
+        [jnp.broadcast_to(bias_ref[s : s + 1, :], (BLOCK, rows)) for s in slots], axis=0
     )
     bias = jnp.concatenate([bias, bias], axis=1)
-    for pair in range(width // LANES):
-        lanes = slice(pair * LANES, (pair + 1) * LANES)
-        queries = head_pair_queries(query_ref[:, lanes])
+    scores = []
+    for lanes in pairs:
+        keys = jnp.concatenate([got[:, lanes] for got in got_refs], axis=0)
+        scores.append(pair_scores(keys, head_pair_queries(query_ref[:, lanes])) + bias)
+    weights, factors, totals = [], [], []
+    for pair in range(len(pairs)):
         peak = peak_ref[pair : pair + 1, :]
-        scores = pair_scores(got_ref[:, lanes], queries) + bias
-        peak_new = jnp.maximum(peak, jnp.max(scores, axis=0, keepdims=True))
+        peak_new = jnp.maximum(peak, jnp.max(scores[pair], axis=0, keepdims=True))
         factor = jnp.exp2((peak - peak_new) * score_factor)
-        weights = jnp.exp2((scores - peak_new) * score_factor)
-        total = total_ref[pair : pair + 1, :] * factor + jnp.sum(weights, axis=0, keepdims=True)
-        values = got_ref[:, width + pair * LANES : width + (pair + 1) * LANES]
-        summed = summed_ref[lanes, :] * widen(factor) + pair_values(
-            values, weights.astype(jnp.bfloat16)
-        )
-        if last:
-            out_refs[0][:, lanes] = (summed / widen(total)).T.astype(jnp.bfloat16)
-        else:
+        weight = jnp.exp2((scores[pair] - peak_new) * score_factor)
+        total = total_ref[pair : pair + 1, :] * factor + jnp.sum(weight, axis=0, keepdims=True)
+        weights.append(weight.astype(jnp.bfloat16))
+        factors.append(factor)
+        totals.append(total)
+        if not last:
             out_refs[0][pair : pair + 1, :] = peak_new
             out_refs[1][pair : pair + 1, :] = total
-            out_refs[2][lanes, :] = summed
+    added = []
+    for pair, lanes in enumerate(spans):
+        values = jnp.concatenate([got[:, lanes] for got in got_refs], axis=0)
+        added.append(pair_values(values, weights[pair]))
+    for pair, lanes in enumerate(pairs):
+        if last:
+            over = 1.0 / totals[pair]
+            summed = summed_ref[lanes, :] * widen(factors[pair] * over) + added[pair] * widen(over)
+            out_refs[0][:, lanes] = summed.T.astype(jnp.bfloat16)
+        else:
+            out_refs[2][lanes, :] = summed_ref[lanes, :] * widen(factors[pair]) + added[pair]
 
 
 def out_own_kernel(own_ref, weight_ref, out_ref):
@@ -297,60 +303,54 @@
     rows, depth = tokens.shape
     width = query_weight.shape[1]
     pairs = width // LANES
-    device = lax.axis_index("kv")
     devices = lax.axis_size("kv")
     swap = [(0, 1), (1, 0)]
 
-    def turn(x, by):
-        return lax.ppermute(x, "kv", [(i, (i + by) % devices) for i in range(devices)])
+    def ask(x, turn):
+        return lax.ppermute(x, "kv", [(i, source_of(i, turn, devices)) for i in range(devices)])
+
+    def send(x, turn):
+        return lax.ppermute(x, "kv", [(source_of(i, turn, devices), i) for i in range(devices)])
 
     other = lax.ppermute(tokens, "tp", swap)
-    asked = []
-    for shift in range(1, devices):
-        asked.append(turn(chosen, -shift))
-    cosine, sine = rotary_tables(device * rows, rows)
-    half = pltpu.VMEM((depth, width), jnp.bfloat16)
-    part, own, key_rest, value_rest = call(
+    asked, turns = [], turn_order(devices)
+    for shift in turns:
+        asked.append(ask(chosen, shift))
+    cosine, sine = rotary_tables(rows)
+    part = call(
         key_value_own_kernel,
         [tokens, key_weight, value_weight],
-        [
-            pltpu.VMEM((rows, 2 * width), jnp.float32),
-            pltpu.VMEM((rows, depth), jnp.bfloat16),
-            half,
-            half,
-        ],
+        [pltpu.VMEM((rows, 2 * width), jnp.float32)],
         flops=4 * rows * depth * width,
-        scratch=[half, half, pltpu.SemaphoreType.DMA((5,))],
-        far=3,
     )
     store = call(
         key_value_kernel,
-        [part, other, key_rest, value_rest, cosine, sine],
+        [part, other, key_weight, value_weight, cosine, sine],
         [pltpu.VMEM((rows, 2 * width), jnp.bfloat16)],
         flops=4 * rows * depth * width,
     )
     got = []
-    for shift in range(1, devices):
+    for shift, asked_by in zip(turns, asked):
         picked = call(
-            pick_kernel,
-            [asked[shift - 1], store],
-            [pltpu.VMEM((CAP * BLOCK, 2 * width), jnp.bfloat16)],
+            pick_kernel, [asked_by, store], [pltpu.VMEM((CAP * BLOCK, 2 * width), jnp.bfloat16)]
         )
-        got.append(turn(picked, shift))
+        got.append(send(picked, shift))
     queries = call(
         query_kernel,
-        [own, other, query_weight, cosine, sine],
+        [tokens, other, query_weight, cosine, sine],
         [pltpu.VMEM((rows, width), jnp.bfloat16)],
         flops=4 * rows * depth * width,
     )
     remote_rows = max(8, (devices - 1) * CAP)
     local_bias, remote_bias = call(
-        functools.partial(list_kernel, devices),
+        functools.partial(list_kernel, devices, turns),
         [chosen],
         [
             pltpu.VMEM((rows // BLOCK, rows), jnp.float32),
             pltpu.VMEM((remote_rows, rows), jnp.float32),
         ],
+        scratch=[pltpu.VMEM(chosen.shape, chosen.dtype), pltpu.SemaphoreType.DMA],
+        far=1,
     )
     state_shapes = [
         pltpu.VMEM((pairs, 2 * rows), jnp.float32),
@@ -361,13 +361,17 @@
     state = call(
         local_kernel, [queries, store, local_bias], state_shapes, flops=16 * rows * rows * width
     )
-    for shift in range(1, devices):
-        last = shift == devices - 1
+    final = max(0, len(got) - 2)
+    groups = [(i, 1) for i in range(final)] + [(final, len(got) - final)]
+    for first, parts in groups:
+        last = first + parts == len(got)
+        if parts == 0:
+            continue
         state = call(
-            functools.partial(remote_kernel, shift, last),
-            [queries, remote_bias, got[shift - 1], *state],
+            functools.partial(remote_kernel, first, parts, last),
+            [queries, remote_bias, *got[first : first + parts], *state],
             attended_shape if last else state_shapes,
-            flops=16 * rows * CAP * BLOCK * width,
+            flops=16 * rows * parts * CAP * BLOCK * width,
         )
     attended = state
     attended_other = lax.ppermute(attended, "tp", swap)

time: 40 us -> 38.6 us (0.965)
  waiting for transfers between devices: 14.9 us -> 6.27 us
  local copies, waits for them, and re-layouts: 0.11 us -> 6.31 us
  starting transfers between devices: 12.6 us -> 16.6 us
  Pallas kernels: 12 us -> 9.01 us
    ppermute x6, waiting for transfers between devices: 13.8 us -> 5.2 us  [the longest x3 5.2 us: ask(): lax.ppermute(x, 'kv', [(i, source_of(i, turn, devices)) for i in range(de...]
    unnamed x6 -> x18, local copies, waits for them, and re-layouts: 0.02 us -> 6.31 us
    ppermute x6, starting transfers between devices: 12 us -> 16 us  [the longest x3 8.5 us: send(): lax.ppermute(x, 'kv', [(source_of(i, turn, devices), i) for i in range(de...]
    pallas_call x14 -> x13, Pallas kernels: 12 us -> 9.01 us  [call(): pl.pallas_call(kernel, in_specs=[VMEM] * near + [anywhere] * far, out_spe...]
  transfers between devices with their start and end apart: 8 -> 8, of which waited for: 4 -> 2; matrix products, arithmetic and copies ran while one was open for 1% -> 0% of each run, Pallas kernels for 23% -> 17%
where the time goes in v2:
time: 38.6 us; the launch traced here: 38.4 us
  starting transfers between devices  16.6 us (43%)
  Pallas kernels  9.01 us (23%)
  local copies, waits for them, and re-layouts  6.31 us (16%)
  waiting for transfers between devices  6.27 us (16%)
    pallas_call x13, Pallas kernels, call(): pl.pallas_call(kernel, in_specs=[VMEM] * near + [anywhere] * far, out_spe...  9.01 us
    ppermute x3, starting transfers between devices, send(): lax.ppermute(x, 'kv', [(source_of(i, turn, devices), i) for i in range(de...  8.5 us
    ppermute x3, starting transfers between devices, ask(): lax.ppermute(x, 'kv', [(i, source_of(i, turn, devices)) for i in range(de...  7.49 us
    unnamed x18, local copies, waits for them, and re-layouts  6.31 us
    ppermute x3, waiting for transfers between devices, ask(): lax.ppermute(x, 'kv', [(i, source_of(i, turn, devices)) for i in range(de...  5.2 us
    ppermute x1, waiting for transfers between devices, on_device(): attended_other = lax.ppermute(attended, 'tp', swap)  1.06 us
  transfers between devices with their start and end apart: 8, of which 2 were waited for; matrix products, arithmetic and copies ran while one was open for 0% of the time, Pallas kernels for 17%

profile of v2, /device:TPU:0, one launch (start us, length us, event | category | flops | bytes accessed | tf_op | source)
XLA Modules:
  0.0 38.4 jit_solution(17558854065536243765)
XLA Ops:
  0.0 0.5 %collective-permute-start = (bf16[256,1024]{1,0:T(8,128)(2,1)}, bf16[256,1024]{1,0:T(8,128)(2,1)S(1)}, u32[]{:S(2)}, u32[]{:S(2)}) collective-permute-start(bf16[256,1024]{1,0:T(8,128)(2,1)} %own_ref.3), channel_id=1, source_target_pairs={{0,1},{1,0},{2,3},{3,2},{4,5},{5,4},{6,7},{7,6},{8,9},{9,8},{10,11... | collective-permute-start | bytes 1572872 | tf_op jit(solution)/shard_map/ppermute | solution.py:315
  0.5 3.6 %collective-permute-start.5 = (s32[8,16]{1,0:T(8,128)}, s32[8,16]{1,0:T(8,128)S(1)}, u32[]{:S(2)}, u32[]{:S(2)}) collective-permute-start(s32[8,16]{1,0:T(8,128)} %far_ref.1), channel_id=1, source_target_pairs={{0,4},{2,6},{4,0},{6,2},{1,5},{3,7},{5,1},{7,3},{8,12},{10,14},{12... | collective-permute-start | bytes 1544 | tf_op jit(solution)/shard_map/ppermute | solution.py:310
  4.1 1.6 %copy-done = bf16[2048,512]{1,0:T(8,128)(2,1)S(1)} copy-done((bf16[2048,512]{1,0:T(8,128)(2,1)S(1)}, bf16[2048,512]{1,0:T(8,128)(2,1)}, u32[]{:S(2)}) %copy-start) | copy-done | bytes 2097176
  5.7 1.6 %copy-done.2 = bf16[2048,512]{1,0:T(8,128)(2,1)S(1)} copy-done((bf16[2048,512]{1,0:T(8,128)(2,1)S(1)}, bf16[2048,512]{1,0:T(8,128)(2,1)}, u32[]{:S(2)}) %copy-start.2) | copy-done | bytes 2097176
  7.3 1.0 %copy-done.6 = bf16[256,1024]{1,0:T(8,128)(2,1)S(1)} copy-done((bf16[256,1024]{1,0:T(8,128)(2,1)S(1)}, bf16[256,1024]{1,0:T(8,128)(2,1)}, u32[]{:S(2)}) %copy-start.6) | copy-done | bytes 524312
  8.3 0.7 %shard_map.67.part_ref = f32[256,1024]{1,0:T(8,128)S(1)} custom-call(bf16[256,1024]{1,0:T(8,128)(2,1)S(1)} %copy-done.6, bf16[2048,512]{1,0:T(8,128)(2,1)S(1)} %copy-done, bf16[2048,512]{1,0:T(8,128)(2,1)S(1)} %copy-done.2), custom_call_target="tpu_custom_call" | custom-call | flops 536870912 | bytes 100000 | tf_op jit(solution)/shard_map/pallas_call | solution.py:37
  9.2 1.4 %copy-done.1 = bf16[2048,512]{1,0:T(8,128)(2,1)S(1)} copy-done((bf16[2048,512]{1,0:T(8,128)(2,1)S(1)}, bf16[2048,512]{1,0:T(8,128)(2,1)}, u32[]{:S(2)}) %copy-start.1) | copy-done | bytes 2097176
  10.6 0.6 %copy-done.3 = bf16[2048,512]{1,0:T(8,128)(2,1)S(1)} copy-done((bf16[2048,512]{1,0:T(8,128)(2,1)S(1)}, bf16[2048,512]{1,0:T(8,128)(2,1)}, u32[]{:S(2)}) %copy-start.3) | copy-done | bytes 2097176
  11.2 0.7 %shard_map.68.store_ref = bf16[256,1024]{1,0:T(8,128)(2,1)S(1)} custom-call(f32[256,1024]{1,0:T(8,128)S(1)} %shard_map.67.part_ref, bf16[256,1024]{1,0:T(8,128)(2,1)S(1)} %collective-permute-done.other_ref, bf16[2048,512]{1,0:T(8,128)(2,1)S(1)} %copy-done.1, bf16[2048,512]{1,0:T(8,128)(2,1)S(1)} %copy-done.3, f32[256,128]{1,0:T(8,128)S(1)} %get-tuple-element.15.cos_ref, ...), custom_call_target="tpu_custom_call" | custom-call | flops 536870912 | bytes 100000 | tf_op jit(solution)/shard_map/pallas_call | solution.py:37
  12.0 0.2 shard_map.71
  12.3 3.9 %collective-permute-start.1 = (s32[8,16]{1,0:T(8,128)S(1)}, s32[8,16]{1,0:T(8,128)S(1)}, u32[]{:S(2)}, u32[]{:S(2)}) collective-permute-start(s32[8,16]{1,0:T(8,128)S(1)} %copy-done.8), channel_id=1, source_target_pairs={{0,6},{2,4},{4,2},{6,0},{1,7},{3,5},{5,3},{7,1},{8,14},{10,12},{12... | collective-permute-start | bytes 1544 | tf_op jit(solution)/shard_map/ppermute | solution.py:310
  16.2 5.2 %collective-permute-done.1.asked_ref = s32[8,16]{1,0:T(8,128)S(1)} collective-permute-done((s32[8,16]{1,0:T(8,128)S(1)}, s32[8,16]{1,0:T(8,128)S(1)}, u32[]{:S(2)}, u32[]{:S(2)}) %collective-permute-start.1) | collective-permute-done | bytes 544 | tf_op jit(solution)/shard_map/ppermute | solution.py:310
  21.4 0.2 shard_map.69
  21.7 0.3 collective-permute-start.2
  22.0 0.2 shard_map.70
  22.2 8.1 %collective-permute-start.4 = (bf16[96,1024]{1,0:T(8,128)(2,1)S(1)}, bf16[96,1024]{1,0:T(8,128)(2,1)S(1)}, u32[]{:S(2)}, u32[]{:S(2)}) collective-permute-start(bf16[96,1024]{1,0:T(8,128)(2,1)S(1)} %shard_map.70), channel_id=1, source_target_pairs={{2,0},{0,2},{6,4},{4,6},{3,1},{1,3},{7,5},{5,7},{10,8},{8,10},{14,... | collective-permute-start | bytes 589832 | tf_op jit(solution)/shard_map/ppermute | solution.py:313
  30.4 1.0 %shard_map.66 = (f32[8,256]{1,0:T(8,128)S(1)}, f32[9,256]{1,0:T(8,128)S(1)}) custom-call(s32[8,16]{1,0:T(8,128)} %far_ref.1), custom_call_target="tpu_custom_call" | custom-call | flops 1000000 | bytes 100000 | tf_op jit(solution)/shard_map/pallas_call | solution.py:37
  31.4 1.0 %shard_map.65.query_ref = bf16[256,512]{1,0:T(8,128)(2,1)S(1)} custom-call(bf16[256,1024]{1,0:T(8,128)(2,1)S(1)} %copy-done.7, bf16[256,1024]{1,0:T(8,128)(2,1)S(1)} %collective-permute-done.other_ref, bf16[2048,512]{1,0:T(8,128)(2,1)S(1)} %copy-done.5, f32[256,128]{1,0:T(8,128)S(1)} %get-tuple-element.15.cos_ref, f32[256,128]{1,0:T(8,128)S(1)} %get-tuple-element.16.sin_ref), custom_call_target="tpu_custom_call" | custom-call | flops 536870912 | bytes 100000 | tf_op jit(solution)/shard_map/pallas_call | solution.py:37
  32.4 1.6 %shard_map.72 = (f32[4,512]{1,0:T(4,128)S(1)}, f32[4,512]{1,0:T(4,128)S(1)}, f32[512,256]{1,0:T(8,128)S(1)}) custom-call(bf16[256,512]{1,0:T(8,128)(2,1)S(1)} %shard_map.65.query_ref, bf16[256,1024]{1,0:T(8,128)(2,1)S(1)} %shard_map.68.store_ref, f32[8,256]{1,0:T(8,128)S(1)} %get-tuple-element.18.bias_ref), custom_call_target="tpu_custom_call" | custom-call | flops 536870912 | bytes 100000 | tf_op jit(solution)/shard_map/pallas_call | solution.py:37
  34.0 0.6 %shard_map.73 = (f32[4,512]{1,0:T(4,128)S(1)}, f32[4,512]{1,0:T(4,128)S(1)}, f32[512,256]{1,0:T(8,128)S(1)}) custom-call(bf16[256,512]{1,0:T(8,128)(2,1)S(1)} %shard_map.65.query_ref, f32[9,256]{1,0:T(8,128)S(1)} %get-tuple-element.17.bias_ref, bf16[96,1024]{1,0:T(8,128)(2,1)S(1)} %collective-permute-done.6.refs_0_, f32[4,512]{1,0:T(4,128)S(1)} %get-tuple-element.19.refs_1_, ...), custom_call_target="tpu_custom_call" | custom-call | flops 201326592 | bytes 100000 | tf_op jit(solution)/shard_map/pallas_call | solution.py:37
  34.7 0.9 %shard_map.74.own_ref = bf16[256,512]{1,0:T(8,128)(2,1)S(1)} custom-call(bf16[256,512]{1,0:T(8,128)(2,1)S(1)} %shard_map.65.query_ref, f32[9,256]{1,0:T(8,128)S(1)} %get-tuple-element.17.bias_ref, bf16[96,1024]{1,0:T(8,128)(2,1)S(1)} %collective-permute-done.2.refs_0_, bf16[96,1024]{1,0:T(8,128)(2,1)S(1)} %collective-permute-done.4.refs_1_, ...), custom_call_target="tpu_custom_call" | custom-call | flops 402653184 | bytes 100000 | tf_op jit(solution)/shard_map/pallas_call | solution.py:37
  35.7 0.4 %shard_map.75.part_ref = f32[256,1024]{1,0:T(8,128)S(1)} custom-call(bf16[256,512]{1,0:T(8,128)(2,1)S(1)} %shard_map.74.own_ref, bf16[1024,1024]{1,0:T(8,128)(2,1)S(1)} %copy-done.4), custom_call_target="tpu_custom_call" | custom-call | flops 268435456 | bytes 100000 | tf_op jit(solution)/shard_map/pallas_call | solution.py:37
  36.1 1.1 %collective-permute-done.7.other_ref = bf16[256,512]{1,0:T(8,128)(2,1)S(1)} collective-permute-done((bf16[256,512]{1,0:T(8,128)(2,1)S(1)}, bf16[256,512]{1,0:T(8,128)(2,1)S(1)}, u32[]{:S(2)}, u32[]{:S(2)}) %collective-permute-start.7) | collective-permute-done | bytes 262176 | tf_op jit(solution)/shard_map/ppermute | solution.py:377
  37.2 1.2 %shard_map.76 = bf16[256,1024]{1,0:T(8,128)(2,1)} custom-call(f32[256,1024]{1,0:T(8,128)S(1)} %shard_map.75.part_ref, bf16[256,512]{1,0:T(8,128)(2,1)S(1)} %collective-permute-done.7.other_ref, bf16[1024,1024]{1,0:T(8,128)(2,1)S(1)} %copy-done.4), custom_call_target="tpu_custom_call" | custom-call | flops 268435456 | bytes 100000 | tf_op jit(solution)/shard_map/pallas_call | solution.py:37
  (23 shorter events, 0.3 us)
Async XLA Ops:
  0.0 9.2 %collective-permute-start = (bf16[256,1024]{1,0:T(8,128)(2,1)}, bf16[256,1024]{1,0:T(8,128)(2,1)S(1)}, u32[]{:S(2)}, u32[]{:S(2)}) collective-permute-start(bf16[256,1024]{1,0:T(8,128)(2,1)} %own_ref.3), channel_id=1, source_target_pairs={{0,1},{1,0},{2,3},{3,2},{4,5},{5,4},{6,7},{7,6},{8,9},{9,8},{10,11... | collective-permute-start | bytes 1572872 | tf_op jit(solution)/shard_map/ppermute | solution.py:315
  0.5 11.5 %collective-permute-start.5 = (s32[8,16]{1,0:T(8,128)}, s32[8,16]{1,0:T(8,128)S(1)}, u32[]{:S(2)}, u32[]{:S(2)}) collective-permute-start(s32[8,16]{1,0:T(8,128)} %far_ref.1), channel_id=1, source_target_pairs={{0,4},{2,6},{4,0},{6,2},{1,5},{3,7},{5,1},{7,3},{8,12},{10,14},{12... | collective-permute-start | bytes 1544 | tf_op jit(solution)/shard_map/ppermute | solution.py:310
  4.1 1.6 %copy-start = (bf16[2048,512]{1,0:T(8,128)(2,1)S(1)}, bf16[2048,512]{1,0:T(8,128)(2,1)}, u32[]{:S(2)}) copy-start(bf16[2048,512]{1,0:T(8,128)(2,1)} %key_ref.3) | copy-start | bytes 6291460
  5.7 1.6 %copy-start.2 = (bf16[2048,512]{1,0:T(8,128)(2,1)S(1)}, bf16[2048,512]{1,0:T(8,128)(2,1)}, u32[]{:S(2)}) copy-start(bf16[2048,512]{1,0:T(8,128)(2,1)} %value_ref.3) | copy-start | bytes 6291460
  7.3 1.0 %copy-start.6 = (bf16[256,1024]{1,0:T(8,128)(2,1)S(1)}, bf16[256,1024]{1,0:T(8,128)(2,1)}, u32[]{:S(2)}) copy-start(bf16[256,1024]{1,0:T(8,128)(2,1)} %own_ref.3) | copy-start | bytes 1572868
  9.0 1.6 %copy-start.1 = (bf16[2048,512]{1,0:T(8,128)(2,1)S(1)}, bf16[2048,512]{1,0:T(8,128)(2,1)}, u32[]{:S(2)}) copy-start(bf16[2048,512]{1,0:T(8,128)(2,1)} %key_ref.3) | copy-start | bytes 6291460
  9.0 2.2 %copy-start.3 = (bf16[2048,512]{1,0:T(8,128)(2,1)S(1)}, bf16[2048,512]{1,0:T(8,128)(2,1)}, u32[]{:S(2)}) copy-start(bf16[2048,512]{1,0:T(8,128)(2,1)} %value_ref.3) | copy-start | bytes 6291460
  11.2 1.1 %copy-start.8 = (s32[8,16]{1,0:T(8,128)S(1)}, s32[8,16]{1,0:T(8,128)}, u32[]{:S(2)}) copy-start(s32[8,16]{1,0:T(8,128)} %far_ref.1) | copy-start | bytes 1540
  11.2 20.2 %copy-start.7 = (bf16[256,1024]{1,0:T(8,128)(2,1)S(1)}, bf16[256,1024]{1,0:T(8,128)(2,1)}, u32[]{:S(2)}) copy-start(bf16[256,1024]{1,0:T(8,128)(2,1)} %own_ref.3) | copy-start | bytes 1572868
  12.0 19.5 %copy-start.5 = (bf16[2048,512]{1,0:T(8,128)(2,1)S(1)}, bf16[2048,512]{1,0:T(8,128)(2,1)}, u32[]{:S(2)}) copy-start(bf16[2048,512]{1,0:T(8,128)(2,1)} %weight_ref.3) | copy-start | bytes 6291460
  12.2 21.8 %collective-permute-start.6 = (bf16[96,1024]{1,0:T(8,128)(2,1)S(1)}, bf16[96,1024]{1,0:T(8,128)(2,1)S(1)}, u32[]{:S(2)}, u32[]{:S(2)}) collective-permute-start(bf16[96,1024]{1,0:T(8,128)(2,1)S(1)} %shard_map.71), channel_id=1, source_target_pairs={{4,0},{6,2},{0,4},{2,6},{5,1},{7,3},{1,5},{3,7},{12,8},{14,10},{8,... | collective-permute-start | bytes 589832 | tf_op jit(solution)/shard_map/ppermute | solution.py:313
  12.3 9.1 %collective-permute-start.1 = (s32[8,16]{1,0:T(8,128)S(1)}, s32[8,16]{1,0:T(8,128)S(1)}, u32[]{:S(2)}, u32[]{:S(2)}) collective-permute-start(s32[8,16]{1,0:T(8,128)S(1)} %copy-done.8), channel_id=1, source_target_pairs={{0,6},{2,4},{4,2},{6,0},{1,7},{3,5},{5,3},{7,1},{8,14},{10,12},{12... | collective-permute-start | bytes 1544 | tf_op jit(solution)/shard_map/ppermute | solution.py:310
  16.2 5.7 %collective-permute-start.3 = (s32[8,16]{1,0:T(8,128)S(1)}, s32[8,16]{1,0:T(8,128)S(1)}, u32[]{:S(2)}, u32[]{:S(2)}) collective-permute-start(s32[8,16]{1,0:T(8,128)S(1)} %copy-done.8), channel_id=1, source_target_pairs={{0,2},{2,0},{4,6},{6,4},{1,3},{3,1},{5,7},{7,5},{8,10},{10,8},{12,... | collective-permute-start | bytes 1544 | tf_op jit(solution)/shard_map/ppermute | solution.py:310
  21.7 13.0 %collective-permute-start.2 = (bf16[96,1024]{1,0:T(8,128)(2,1)S(1)}, bf16[96,1024]{1,0:T(8,128)(2,1)S(1)}, u32[]{:S(2)}, u32[]{:S(2)}) collective-permute-start(bf16[96,1024]{1,0:T(8,128)(2,1)S(1)} %shard_map.69), channel_id=1, source_target_pairs={{6,0},{4,2},{2,4},{0,6},{7,1},{5,3},{3,5},{1,7},{14,8},{12,10},{10... | collective-permute-start | bytes 589832 | tf_op jit(solution)/shard_map/ppermute | solution.py:313
  22.2 12.5 %collective-permute-start.4 = (bf16[96,1024]{1,0:T(8,128)(2,1)S(1)}, bf16[96,1024]{1,0:T(8,128)(2,1)S(1)}, u32[]{:S(2)}, u32[]{:S(2)}) collective-permute-start(bf16[96,1024]{1,0:T(8,128)(2,1)S(1)} %shard_map.70), channel_id=1, source_target_pairs={{2,0},{0,2},{6,4},{4,6},{3,1},{1,3},{7,5},{5,7},{10,8},{8,10},{14,... | collective-permute-start | bytes 589832 | tf_op jit(solution)/shard_map/ppermute | solution.py:313
  32.4 3.2 %copy-start.4 = (bf16[1024,1024]{1,0:T(8,128)(2,1)S(1)}, bf16[1024,1024]{1,0:T(8,128)(2,1)}, u32[]{:S(2)}) copy-start(bf16[1024,1024]{1,0:T(8,128)(2,1)} %weight_ref.5) | copy-start | bytes 6291460
  35.6 1.6 %collective-permute-start.7 = (bf16[256,512]{1,0:T(8,128)(2,1)S(1)}, bf16[256,512]{1,0:T(8,128)(2,1)S(1)}, u32[]{:S(2)}, u32[]{:S(2)}) collective-permute-start(bf16[256,512]{1,0:T(8,128)(2,1)S(1)} %shard_map.74.own_ref), channel_id=1, source_target_pairs={{0,1},{1,0},{2,3},{3,2},{4,5},{5,4},{6,7},{7,6},{8,9},{9,8},{10,11... | collective-permute-start | bytes 786440 | tf_op jit(solution)/shard_map/ppermute | solution.py:377

commit v3 on v2

--- a/solution.py
+++ b/solution.py
@@ -28,7 +28,8 @@
 
 
 def turn_order(devices):
-    return [*range(2, devices), 1] if devices > 1 else []
+    last = devices - 1
+    return [*range(2, last), *([1] if last > 1 else []), last]
 
 
 def call(kernel, operands, results, flops=1000000, limit=16, scratch=(), far=0):
@@ -125,8 +126,9 @@
         out_ref[:, lanes] = rotate(acc[:, lanes], cosine, sine).astype(jnp.bfloat16)
 
 
-def pick_kernel(asked_ref, store_ref, out_ref):
+def pick_kernel(cuts, asked_ref, store_ref, *out_refs):
     blocks = store_ref.shape[0] // BLOCK
+    width = store_ref.shape[1] // 2
     first = lax.axis_index("kv") * blocks
     asked = asked_ref[...]
     count = jnp.int32(0)
@@ -136,9 +138,12 @@
         for slot in range(CAP):
             index[slot] = jnp.where((hit == 1) & (count == slot), block, index[slot])
         count = count + hit
-    for slot in range(CAP):
-        rows = pl.ds(pl.multiple_of(index[slot] * BLOCK, BLOCK), BLOCK)
-        out_ref[slot * BLOCK : (slot + 1) * BLOCK, :] = store_ref[rows, :]
+    for (low, high), out_ref in zip(cuts, out_refs):
+        for slot in range(CAP):
+            rows = pl.ds(pl.multiple_of(index[slot] * BLOCK, BLOCK), BLOCK)
+            place = slice(slot * BLOCK, (slot + 1) * BLOCK)
+            out_ref[place, : high - low] = store_ref[rows, low:high]
+            out_ref[place, high - low :] = store_ref[rows, width + low : width + high]
 
 
 def list_kernel(devices, turns, far_ref, local_ref, remote_ref, chosen_ref, sem):
@@ -237,55 +242,75 @@
         summed_ref[lanes, :] = pair_values(values, weights.astype(jnp.bfloat16))
 
 
-def remote_kernel(first, parts, last, query_ref, bias_ref, *refs):
-    got_refs, (peak_ref, total_ref, summed_ref) = refs[:parts], refs[parts : parts + 3]
-    out_refs = refs[parts + 3 :]
-    rows, width = query_ref.shape
-    pairs = [slice(p * LANES, (p + 1) * LANES) for p in range(width // LANES)]
-    spans = [slice(width + p.start, width + p.stop) for p in pairs]
-    slots = range(first * CAP, (first + parts) * CAP)
+def remote_kernel(place, low, last, query_ref, bias_ref, got_ref, *refs):
+    (peak_ref, total_ref, summed_ref), out_refs = refs[:3], refs[3:]
+    rows = query_ref.shape[0]
+    width = got_ref.shape[1] // 2
+    count = width // LANES
     bias = jnp.concatenate(
-        [jnp.broadcast_to(bias_ref[s : s + 1, :], (BLOCK, rows)) for s in slots], axis=0
+        [
+            jnp.broadcast_to(bias_ref[s : s + 1, :], (BLOCK, rows))
+            for s in range(place * CAP, (place + 1) * CAP)
+        ],
+        axis=0,
     )
     bias = jnp.concatenate([bias, bias], axis=1)
-    scores = []
-    for lanes in pairs:
-        keys = jnp.concatenate([got[:, lanes] for got in got_refs], axis=0)
-        scores.append(pair_scores(keys, head_pair_queries(query_ref[:, lanes])) + bias)
+    here = [slice(p * LANES, (p + 1) * LANES) for p in range(count)]
+    lanes = [slice(low + h.start, low + h.stop) for h in here]
+    stats = [low // LANES + p for p in range(count)]
+    scores = [
+        pair_scores(got_ref[:, here[p]], head_pair_queries(query_ref[:, lanes[p]])) + bias
+        for p in range(count)
+    ]
     weights, factors, totals = [], [], []
-    for pair in range(len(pairs)):
-        peak = peak_ref[pair : pair + 1, :]
-        peak_new = jnp.maximum(peak, jnp.max(scores[pair], axis=0, keepdims=True))
+    for p, at in enumerate(stats):
+        peak = peak_ref[at : at + 1, :]
+        peak_new = jnp.maximum(peak, jnp.max(scores[p], axis=0, keepdims=True))
         factor = jnp.exp2((peak - peak_new) * score_factor)
-        weight = jnp.exp2((scores[pair] - peak_new) * score_factor)
-        total = total_ref[pair : pair + 1, :] * factor + jnp.sum(weight, axis=0, keepdims=True)
+        weight = jnp.exp2((scores[p] - peak_new) * score_factor)
+        total = total_ref[at : at + 1, :] * factor + jnp.sum(weight, axis=0, keepdims=True)
         weights.append(weight.astype(jnp.bfloat16))
         factors.append(factor)
         totals.append(total)
         if not last:
-            out_refs[0][pair : pair + 1, :] = peak_new
-            out_refs[1][pair : pair + 1, :] = total
-    added = []
-    for pair, lanes in enumerate(spans):
-        values = jnp.concatenate([got[:, lanes] for got in got_refs], axis=0)
-        added.append(pair_values(values, weights[pair]))
-    for pair, lanes in enumerate(pairs):
+            out_refs[0][at : at + 1, :] = peak_new
+            out_refs[1][at : at + 1, :] = total
+    added = [
+        pair_values(got_ref[:, width + here[p].start : width + here[p].stop], weights[p])
+        for p in range(count)
+    ]
+    for p in range(count):
         if last:
-            over = 1.0 / totals[pair]
-            summed = summed_ref[lanes, :] * widen(factors[pair] * over) + added[pair] * widen(over)
-            out_refs[0][:, lanes] = summed.T.astype(jnp.bfloat16)
+            over = 1.0 / totals[p]
+            summed = summed_ref[lanes[p], :] * widen(factors[p] * over) + added[p] * widen(over)
+            out_refs[0][:, here[p]] = summed.T.astype(jnp.bfloat16)
         else:
-            out_refs[2][lanes, :] = summed_ref[lanes, :] * widen(factors[pair]) + added[pair]
-
-
-def out_own_kernel(own_ref, weight_ref, out_ref):
-    out_ref[...] = dot(own_ref[...], weight_ref[half_rows(weight_ref, False), :])
-
-
-def out_kernel(part_ref, other_ref, weight_ref, out_ref, tile_ref, sems):
+            out_refs[2][lanes[p], :] = summed_ref[lanes[p], :] * widen(factors[p]) + added[p]
+
+
+def head_rows(weight_ref, other, low, width):
+    mine = lax.axis_index("tp")
+    depth = weight_ref.shape[0] // 2
+    half = 1 - mine if other else mine
+    return pl.ds(pl.multiple_of(half * depth + low, LANES), width)
+
+
+def out_first_kernel(own_ref, other_ref, weight_ref, out_ref):
+    width = own_ref.shape[1]
+    out_ref[...] = dot(own_ref[...], weight_ref[head_rows(weight_ref, False, 0, width), :]) + dot(
+        other_ref[...], weight_ref[head_rows(weight_ref, True, 0, width), :]
+    )
+
+
+def out_own_kernel(low, part_ref, own_ref, weight_ref, out_ref):
+    rows = head_rows(weight_ref, False, low, own_ref.shape[1])
+    out_ref[...] = part_ref[...] + dot(own_ref[...], weight_ref[rows, :])
+
+
+def out_kernel(low, part_ref, other_ref, weight_ref, out_ref, tile_ref, sems):
     tiles = tile_ref.shape[0]
     width = tile_ref.shape[2]
-    rows = half_rows(weight_ref, True)
+    rows = head_rows(weight_ref, True, low, other_ref.shape[1])
     copies = []
     for tile in range(tiles):
         lanes = slice(tile * width, (tile + 1) * width)
@@ -314,8 +339,8 @@
 
     other = lax.ppermute(tokens, "tp", swap)
     asked, turns = [], turn_order(devices)
-    for shift in turns:
-        asked.append(ask(chosen, shift))
+    for turn in turns:
+        asked.append(ask(chosen, turn))
     cosine, sine = rotary_tables(rows)
     part = call(
         key_value_own_kernel,
@@ -329,12 +354,18 @@
         [pltpu.VMEM((rows, 2 * width), jnp.bfloat16)],
         flops=4 * rows * depth * width,
     )
+    cut = width // 2
+    cuts = [(0, cut), (cut, width)]
     got = []
-    for shift, asked_by in zip(turns, asked):
+    for turn, asked_by in zip(turns, asked):
+        parts = cuts if turn == turns[-1] else [(0, width)]
         picked = call(
-            pick_kernel, [asked_by, store], [pltpu.VMEM((CAP * BLOCK, 2 * width), jnp.bfloat16)]
+            functools.partial(pick_kernel, parts),
+            [asked_by, store],
+            [pltpu.VMEM((CAP * BLOCK, 2 * (high - low)), jnp.bfloat16) for low, high in parts],
         )
-        got.append(send(picked, shift))
+        for part, block in enumerate(picked if len(parts) > 1 else [picked]):
+            got.append(send(block, turn))
     queries = call(
         query_kernel,
         [tokens, other, query_weight, cosine, sine],
@@ -357,37 +388,48 @@
         pltpu.VMEM((pairs, 2 * rows), jnp.float32),
         pltpu.VMEM((width, rows), jnp.float32),
     ]
-    attended_shape = [pltpu.VMEM((rows, width), jnp.bfloat16)]
     state = call(
         local_kernel, [queries, store, local_bias], state_shapes, flops=16 * rows * rows * width
     )
-    final = max(0, len(got) - 2)
-    groups = [(i, 1) for i in range(final)] + [(final, len(got) - final)]
-    for first, parts in groups:
-        last = first + parts == len(got)
-        if parts == 0:
-            continue
+    for place in range(len(turns) - 1):
         state = call(
-            functools.partial(remote_kernel, first, parts, last),
-            [queries, remote_bias, *got[first : first + parts], *state],
-            attended_shape if last else state_shapes,
-            flops=16 * rows * parts * CAP * BLOCK * width,
+            functools.partial(remote_kernel, place, 0, False),
+            [queries, remote_bias, got[place], *state],
+            state_shapes,
+            flops=16 * rows * CAP * BLOCK * width,
         )
-    attended = state
-    attended_other = lax.ppermute(attended, "tp", swap)
+    attended, swapped = [], []
+    for part, (low, high) in enumerate(cuts):
+        attended.append(
+            call(
+                functools.partial(remote_kernel, len(turns) - 1, low, True),
+                [queries, remote_bias, got[len(turns) - 1 + part], *state],
+                [pltpu.VMEM((rows, high - low), jnp.bfloat16)],
+                flops=16 * rows * CAP * BLOCK * (high - low),
+            )
+        )
+        swapped.append(lax.ppermute(attended[part], "tp", swap))
     out_width = out_weight.shape[1]
+    part_shape = [pltpu.VMEM((rows, out_width), jnp.float32)]
+    low = cuts[1][0]
+    out_first = call(
+        out_first_kernel,
+        [attended[0], swapped[0], out_weight],
+        part_shape,
+        flops=4 * rows * low * out_width,
+    )
     out_part = call(
-        out_own_kernel,
-        [attended, out_weight],
-        [pltpu.VMEM((rows, out_width), jnp.float32)],
-        flops=2 * rows * width * out_width,
+        functools.partial(out_own_kernel, low),
+        [out_first, attended[1], out_weight],
+        part_shape,
+        flops=2 * rows * (width - low) * out_width,
     )
     tiles = 4
     return call(
-        out_kernel,
-        [out_part, attended_other, out_weight],
+        functools.partial(out_kernel, low),
+        [out_part, swapped[1], out_weight],
         [pltpu.HBM((rows, out_width), jnp.bfloat16)],
-        flops=2 * rows * width * out_width,
+        flops=2 * rows * (width - low) * out_width,
         scratch=[
             pltpu.VMEM((tiles, rows, out_width // tiles), jnp.bfloat16),
             pltpu.SemaphoreType.DMA((tiles,)),

time: 38.6 us -> 40 us (1.036)
  Pallas kernels: 9.01 us -> 10 us
    ppermute x3 -> x4, starting transfers between devices: 8.5 us -> 6.51 us  [send(): lax.ppermute(x, 'kv', [(source_of(i, turn, devices), i) for i in range(de...]
    ppermute x3, starting transfers between devices: 7.49 us -> 9.12 us  [ask(): lax.ppermute(x, 'kv', [(i, source_of(i, turn, devices)) for i in range(de...]
    pallas_call x13 -> x16, Pallas kernels: 9.01 us -> 10 us  [call(): pl.pallas_call(kernel, in_specs=[VMEM] * near + [anywhere] * far, out_spe...]
    ppermute x3, waiting for transfers between devices: 5.2 us -> 6.05 us  [ask(): lax.ppermute(x, 'kv', [(i, source_of(i, turn, devices)) for i in range(de...]
    ppermute x1 -> x2, waiting for transfers between devices: 1.06 us -> 0.23 us  [on_device(): swapped.append(lax.ppermute(attended[part], 'tp', swap))]
    ppermute x1 -> x2, starting transfers between devices: 0.07 us -> 0.63 us  [on_device(): swapped.append(lax.ppermute(attended[part], 'tp', swap))]
  transfers between devices with their start and end apart: 8 -> 10, of which waited for: 2 -> 4; matrix products, arithmetic and copies ran while one was open for 0% -> 0% of each run, Pallas kernels for 17% -> 22%
where the time goes in v3:
time: 40 us; the launch traced here: 39.7 us
  starting transfers between devices  16.7 us (42%)
  Pallas kernels  10 us (25%)
  waiting for transfers between devices  6.46 us (16%)
  local copies, waits for them, and re-layouts  6.31 us (16%)
    pallas_call x16, Pallas kernels, call(): pl.pallas_call(kernel, in_specs=[VMEM] * near + [anywhere] * far, out_spe...  10 us
    ppermute x3, starting transfers between devices, ask(): lax.ppermute(x, 'kv', [(i, source_of(i, turn, devices)) for i in range(de...  9.12 us
    ppermute x4, starting transfers between devices, send(): lax.ppermute(x, 'kv', [(source_of(i, turn, devices), i) for i in range(de...  6.51 us
    unnamed x18, local copies, waits for them, and re-layouts  6.31 us
    ppermute x3, waiting for transfers between devices, ask(): lax.ppermute(x, 'kv', [(i, source_of(i, turn, devices)) for i in range(de...  6.05 us
  transfers between devices with their start and end apart: 10, of which 4 were waited for; matrix products, arithmetic and copies ran while one was open for 0% of the time, Pallas kernels for 22%

profile of v3, /device:TPU:0, one launch (start us, length us, event | category | flops | bytes accessed | tf_op | source)
XLA Modules:
  0.0 39.7 jit_solution(3604914309593852880)
XLA Ops:
  0.5 3.6 %collective-permute-start.5 = (s32[8,16]{1,0:T(8,128)}, s32[8,16]{1,0:T(8,128)S(1)}, u32[]{:S(2)}, u32[]{:S(2)}) collective-permute-start(s32[8,16]{1,0:T(8,128)} %far_ref.1), channel_id=1, source_target_pairs={{0,4},{2,6},{4,0},{6,2},{1,5},{3,7},{5,1},{7,3},{8,12},{10,14},{12... | collective-permute-start | bytes 1544 | tf_op jit(solution)/shard_map/ppermute | solution.py:335
  4.1 1.6 %copy-done.1 = bf16[2048,512]{1,0:T(8,128)(2,1)S(1)} copy-done((bf16[2048,512]{1,0:T(8,128)(2,1)S(1)}, bf16[2048,512]{1,0:T(8,128)(2,1)}, u32[]{:S(2)}) %copy-start.1) | copy-done | bytes 2097176
  5.7 1.6 %copy-done.3 = bf16[2048,512]{1,0:T(8,128)(2,1)S(1)} copy-done((bf16[2048,512]{1,0:T(8,128)(2,1)S(1)}, bf16[2048,512]{1,0:T(8,128)(2,1)}, u32[]{:S(2)}) %copy-start.3) | copy-done | bytes 2097176
  7.3 1.0 %copy-done.6 = bf16[256,1024]{1,0:T(8,128)(2,1)S(1)} copy-done((bf16[256,1024]{1,0:T(8,128)(2,1)S(1)}, bf16[256,1024]{1,0:T(8,128)(2,1)}, u32[]{:S(2)}) %copy-start.6) | copy-done | bytes 524312
  8.3 0.7 %shard_map.67.part_ref = f32[256,1024]{1,0:T(8,128)S(1)} custom-call(bf16[256,1024]{1,0:T(8,128)(2,1)S(1)} %copy-done.6, bf16[2048,512]{1,0:T(8,128)(2,1)S(1)} %copy-done.1, bf16[2048,512]{1,0:T(8,128)(2,1)S(1)} %copy-done.3), custom_call_target="tpu_custom_call" | custom-call | flops 536870912 | bytes 100000 | tf_op jit(solution)/shard_map/pallas_call | solution.py:38
  9.2 1.4 %copy-done.2 = bf16[2048,512]{1,0:T(8,128)(2,1)S(1)} copy-done((bf16[2048,512]{1,0:T(8,128)(2,1)S(1)}, bf16[2048,512]{1,0:T(8,128)(2,1)}, u32[]{:S(2)}) %copy-start.2) | copy-done | bytes 2097176
  10.6 0.6 %copy-done.4 = bf16[2048,512]{1,0:T(8,128)(2,1)S(1)} copy-done((bf16[2048,512]{1,0:T(8,128)(2,1)S(1)}, bf16[2048,512]{1,0:T(8,128)(2,1)}, u32[]{:S(2)}) %copy-start.4) | copy-done | bytes 2097176
  11.2 0.7 %shard_map.68.store_ref = bf16[256,1024]{1,0:T(8,128)(2,1)S(1)} custom-call(f32[256,1024]{1,0:T(8,128)S(1)} %shard_map.67.part_ref, bf16[256,1024]{1,0:T(8,128)(2,1)S(1)} %collective-permute-done.other_ref, bf16[2048,512]{1,0:T(8,128)(2,1)S(1)} %copy-done.2, bf16[2048,512]{1,0:T(8,128)(2,1)S(1)} %copy-done.4, f32[256,128]{1,0:T(8,128)S(1)} %get-tuple-element.20.cos_ref, ...), custom_call_target="tpu_custom_call" | custom-call | flops 536870912 | bytes 100000 | tf_op jit(solution)/shard_map/pallas_call | solution.py:38
  12.3 1.9 %collective-permute-start.3 = (s32[8,16]{1,0:T(8,128)S(1)}, s32[8,16]{1,0:T(8,128)S(1)}, u32[]{:S(2)}, u32[]{:S(2)}) collective-permute-start(s32[8,16]{1,0:T(8,128)S(1)} %copy-done.8), channel_id=1, source_target_pairs={{0,2},{2,0},{4,6},{6,4},{1,3},{3,1},{5,7},{7,5},{8,10},{10,8},{12,... | collective-permute-start | bytes 1544 | tf_op jit(solution)/shard_map/ppermute | solution.py:335
  14.2 3.1 %collective-permute-done.3.asked_ref = s32[8,16]{1,0:T(8,128)S(1)} collective-permute-done((s32[8,16]{1,0:T(8,128)S(1)}, s32[8,16]{1,0:T(8,128)S(1)}, u32[]{:S(2)}, u32[]{:S(2)}) %collective-permute-start.3) | collective-permute-done | bytes 544 | tf_op jit(solution)/shard_map/ppermute | solution.py:335
  17.5 2.5 %collective-permute-start.4 = (bf16[96,1024]{1,0:T(8,128)(2,1)S(1)}, bf16[96,1024]{1,0:T(8,128)(2,1)S(1)}, u32[]{:S(2)}, u32[]{:S(2)}) collective-permute-start(bf16[96,1024]{1,0:T(8,128)(2,1)S(1)} %shard_map.70), channel_id=1, source_target_pairs={{2,0},{0,2},{6,4},{4,6},{3,1},{1,3},{7,5},{5,7},{10,8},{8,10},{14,... | collective-permute-start | bytes 589832 | tf_op jit(solution)/shard_map/ppermute | solution.py:338
  20.1 3.7 %collective-permute-start.1 = (s32[8,16]{1,0:T(8,128)S(1)}, s32[8,16]{1,0:T(8,128)S(1)}, u32[]{:S(2)}, u32[]{:S(2)}) collective-permute-start(s32[8,16]{1,0:T(8,128)S(1)} %copy-done.8), channel_id=1, source_target_pairs={{0,6},{2,4},{4,2},{6,0},{1,7},{3,5},{5,3},{7,1},{8,14},{10,12},{12... | collective-permute-start | bytes 1544 | tf_op jit(solution)/shard_map/ppermute | solution.py:335
  23.7 1.0 %shard_map.66 = (f32[8,256]{1,0:T(8,128)S(1)}, f32[9,256]{1,0:T(8,128)S(1)}) custom-call(s32[8,16]{1,0:T(8,128)} %far_ref.1), custom_call_target="tpu_custom_call" | custom-call | flops 1000000 | bytes 100000 | tf_op jit(solution)/shard_map/pallas_call | solution.py:38
  24.8 3.0 %collective-permute-done.1.asked_ref = s32[8,16]{1,0:T(8,128)S(1)} collective-permute-done((s32[8,16]{1,0:T(8,128)S(1)}, s32[8,16]{1,0:T(8,128)S(1)}, u32[]{:S(2)}, u32[]{:S(2)}) %collective-permute-start.1) | collective-permute-done | bytes 544 | tf_op jit(solution)/shard_map/ppermute | solution.py:335
  28.0 1.5 %collective-permute-start.8 = (bf16[96,512]{1,0:T(8,128)(2,1)S(1)}, bf16[96,512]{1,0:T(8,128)(2,1)S(1)}, u32[]{:S(2)}, u32[]{:S(2)}) collective-permute-start(bf16[96,512]{1,0:T(8,128)(2,1)S(1)} %get-tuple-element.34), channel_id=1, source_target_pairs={{6,0},{4,2},{2,4},{0,6},{7,1},{5,3},{3,5},{1,7},{14,8},{12,10},{10... | collective-permute-start | bytes 294920 | tf_op jit(solution)/shard_map/ppermute | solution.py:338
  29.5 2.4 %collective-permute-start.2 = (bf16[96,512]{1,0:T(8,128)(2,1)S(1)}, bf16[96,512]{1,0:T(8,128)(2,1)S(1)}, u32[]{:S(2)}, u32[]{:S(2)}) collective-permute-start(bf16[96,512]{1,0:T(8,128)(2,1)S(1)} %get-tuple-element.23), channel_id=1, source_target_pairs={{6,0},{4,2},{2,4},{0,6},{7,1},{5,3},{3,5},{1,7},{14,8},{12,10},{10... | collective-permute-start | bytes 294920 | tf_op jit(solution)/shard_map/ppermute | solution.py:338
  31.9 1.0 %shard_map.65.query_ref = bf16[256,512]{1,0:T(8,128)(2,1)S(1)} custom-call(bf16[256,1024]{1,0:T(8,128)(2,1)S(1)} %copy-done.7, bf16[256,1024]{1,0:T(8,128)(2,1)S(1)} %collective-permute-done.other_ref, bf16[2048,512]{1,0:T(8,128)(2,1)S(1)} %copy-done.5, f32[256,128]{1,0:T(8,128)S(1)} %get-tuple-element.20.cos_ref, f32[256,128]{1,0:T(8,128)S(1)} %get-tuple-element.21.sin_ref), custom_call_target="tpu_custom_call" | custom-call | flops 536870912 | bytes 100000 | tf_op jit(solution)/shard_map/pallas_call | solution.py:38
  32.9 1.6 %shard_map.72 = (f32[4,512]{1,0:T(4,128)S(1)}, f32[4,512]{1,0:T(4,128)S(1)}, f32[512,256]{1,0:T(8,128)S(1)}) custom-call(bf16[256,512]{1,0:T(8,128)(2,1)S(1)} %shard_map.65.query_ref, bf16[256,1024]{1,0:T(8,128)(2,1)S(1)} %shard_map.68.store_ref, f32[8,256]{1,0:T(8,128)S(1)} %get-tuple-element.24.bias_ref), custom_call_target="tpu_custom_call" | custom-call | flops 536870912 | bytes 100000 | tf_op jit(solution)/shard_map/pallas_call | solution.py:38
  34.5 0.6 %shard_map.73 = (f32[4,512]{1,0:T(4,128)S(1)}, f32[4,512]{1,0:T(4,128)S(1)}, f32[512,256]{1,0:T(8,128)S(1)}) custom-call(bf16[256,512]{1,0:T(8,128)(2,1)S(1)} %shard_map.65.query_ref, f32[9,256]{1,0:T(8,128)S(1)} %get-tuple-element.22.bias_ref, bf16[96,1024]{1,0:T(8,128)(2,1)S(1)} %collective-permute-done.6.got_ref, f32[4,512]{1,0:T(4,128)S(1)} %get-tuple-element.25.refs_0_, ...), custom_call_target="tpu_custom_call" | custom-call | flops 201326592 | bytes 100000 | tf_op jit(solution)/shard_map/pallas_call | solution.py:38
  35.1 0.6 %shard_map.74 = (f32[4,512]{1,0:T(4,128)S(1)}, f32[4,512]{1,0:T(4,128)S(1)}, f32[512,256]{1,0:T(8,128)S(1)}) custom-call(bf16[256,512]{1,0:T(8,128)(2,1)S(1)} %shard_map.65.query_ref, f32[9,256]{1,0:T(8,128)S(1)} %get-tuple-element.22.bias_ref, bf16[96,1024]{1,0:T(8,128)(2,1)S(1)} %collective-permute-done.4.got_ref, f32[4,512]{1,0:T(4,128)S(1)} %get-tuple-element.28.refs_0_, ...), custom_call_target="tpu_custom_call" | custom-call | flops 201326592 | bytes 100000 | tf_op jit(solution)/shard_map/pallas_call | solution.py:38
  35.9 0.5 %shard_map.75.own_ref = bf16[256,256]{1,0:T(8,128)(2,1)S(1)} custom-call(bf16[256,512]{1,0:T(8,128)(2,1)S(1)} %shard_map.65.query_ref, f32[9,256]{1,0:T(8,128)S(1)} %get-tuple-element.22.bias_ref, bf16[96,512]{1,0:T(8,128)(2,1)S(1)} %collective-permute-done.2.got_ref, f32[4,512]{1,0:T(4,128)S(1)} %get-tuple-element.31.refs_0_, ...), custom_call_target="tpu_custom_call" | custom-call | flops 100663296 | bytes 100000 | tf_op jit(solution)/shard_map/pallas_call | solution.py:38
  36.6 0.5 %shard_map.77.own_ref = bf16[256,256]{1,0:T(8,128)(2,1)S(1)} custom-call(bf16[256,512]{1,0:T(8,128)(2,1)S(1)} %shard_map.65.query_ref, f32[9,256]{1,0:T(8,128)S(1)} %get-tuple-element.22.bias_ref, bf16[96,512]{1,0:T(8,128)(2,1)S(1)} %collective-permute-done.8.got_ref, f32[4,512]{1,0:T(4,128)S(1)} %get-tuple-element.31.refs_0_, ...), custom_call_target="tpu_custom_call" | custom-call | flops 100663296 | bytes 100000 | tf_op jit(solution)/shard_map/pallas_call | solution.py:38
  37.1 0.6 %collective-permute-start.9 = (bf16[256,256]{1,0:T(8,128)(2,1)S(1)}, bf16[256,256]{1,0:T(8,128)(2,1)S(1)}, u32[]{:S(2)}, u32[]{:S(2)}) collective-permute-start(bf16[256,256]{1,0:T(8,128)(2,1)S(1)} %shard_map.77.own_ref), channel_id=1, source_target_pairs={{0,1},{1,0},{2,3},{3,2},{4,5},{5,4},{6,7},{7,6},{8,9},{9,8},{10,11... | collective-permute-start | bytes 393224 | tf_op jit(solution)/shard_map/ppermute | solution.py:411
  38.7 1.1 %shard_map.79 = bf16[256,1024]{1,0:T(8,128)(2,1)} custom-call(f32[256,1024]{1,0:T(8,128)S(1)} %shard_map.78.part_ref, bf16[256,256]{1,0:T(8,128)(2,1)S(1)} %collective-permute-done.9.other_ref, bf16[1024,1024]{1,0:T(8,128)(2,1)S(1)} %copy-done), custom_call_target="tpu_custom_call" | custom-call | flops 134217728 | bytes 100000 | tf_op jit(solution)/shard_map/pallas_call | solution.py:38
  (30 shorter events, 2.7 us)
Async XLA Ops:
  0.0 9.2 %collective-permute-start = (bf16[256,1024]{1,0:T(8,128)(2,1)}, bf16[256,1024]{1,0:T(8,128)(2,1)S(1)}, u32[]{:S(2)}, u32[]{:S(2)}) collective-permute-start(bf16[256,1024]{1,0:T(8,128)(2,1)} %own_ref.3), channel_id=1, source_target_pairs={{0,1},{1,0},{2,3},{3,2},{4,5},{5,4},{6,7},{7,6},{8,9},{9,8},{10,11... | collective-permute-start | bytes 1572872 | tf_op jit(solution)/shard_map/ppermute | solution.py:340
  0.5 11.5 %collective-permute-start.5 = (s32[8,16]{1,0:T(8,128)}, s32[8,16]{1,0:T(8,128)S(1)}, u32[]{:S(2)}, u32[]{:S(2)}) collective-permute-start(s32[8,16]{1,0:T(8,128)} %far_ref.1), channel_id=1, source_target_pairs={{0,4},{2,6},{4,0},{6,2},{1,5},{3,7},{5,1},{7,3},{8,12},{10,14},{12... | collective-permute-start | bytes 1544 | tf_op jit(solution)/shard_map/ppermute | solution.py:335
  4.1 1.6 %copy-start.1 = (bf16[2048,512]{1,0:T(8,128)(2,1)S(1)}, bf16[2048,512]{1,0:T(8,128)(2,1)}, u32[]{:S(2)}) copy-start(bf16[2048,512]{1,0:T(8,128)(2,1)} %key_ref.3) | copy-start | bytes 6291460
  5.7 1.6 %copy-start.3 = (bf16[2048,512]{1,0:T(8,128)(2,1)S(1)}, bf16[2048,512]{1,0:T(8,128)(2,1)}, u32[]{:S(2)}) copy-start(bf16[2048,512]{1,0:T(8,128)(2,1)} %value_ref.3) | copy-start | bytes 6291460
  7.3 1.0 %copy-start.6 = (bf16[256,1024]{1,0:T(8,128)(2,1)S(1)}, bf16[256,1024]{1,0:T(8,128)(2,1)}, u32[]{:S(2)}) copy-start(bf16[256,1024]{1,0:T(8,128)(2,1)} %own_ref.3) | copy-start | bytes 1572868
  9.0 1.6 %copy-start.2 = (bf16[2048,512]{1,0:T(8,128)(2,1)S(1)}, bf16[2048,512]{1,0:T(8,128)(2,1)}, u32[]{:S(2)}) copy-start(bf16[2048,512]{1,0:T(8,128)(2,1)} %key_ref.3) | copy-start | bytes 6291460
  9.0 2.2 %copy-start.4 = (bf16[2048,512]{1,0:T(8,128)(2,1)S(1)}, bf16[2048,512]{1,0:T(8,128)(2,1)}, u32[]{:S(2)}) copy-start(bf16[2048,512]{1,0:T(8,128)(2,1)} %value_ref.3) | copy-start | bytes 6291460
  11.2 1.1 %copy-start.8 = (s32[8,16]{1,0:T(8,128)S(1)}, s32[8,16]{1,0:T(8,128)}, u32[]{:S(2)}) copy-start(s32[8,16]{1,0:T(8,128)} %far_ref.1) | copy-start | bytes 1540
  11.2 20.7 %copy-start.5 = (bf16[2048,512]{1,0:T(8,128)(2,1)S(1)}, bf16[2048,512]{1,0:T(8,128)(2,1)}, u32[]{:S(2)}) copy-start(bf16[2048,512]{1,0:T(8,128)(2,1)} %weight_ref.4) | copy-start | bytes 6291460
  12.0 19.9 %copy-start.7 = (bf16[256,1024]{1,0:T(8,128)(2,1)S(1)}, bf16[256,1024]{1,0:T(8,128)(2,1)}, u32[]{:S(2)}) copy-start(bf16[256,1024]{1,0:T(8,128)(2,1)} %own_ref.3) | copy-start | bytes 1572868
  12.2 22.3 %collective-permute-start.6 = (bf16[96,1024]{1,0:T(8,128)(2,1)S(1)}, bf16[96,1024]{1,0:T(8,128)(2,1)S(1)}, u32[]{:S(2)}, u32[]{:S(2)}) collective-permute-start(bf16[96,1024]{1,0:T(8,128)(2,1)S(1)} %shard_map.71), channel_id=1, source_target_pairs={{4,0},{6,2},{0,4},{2,6},{5,1},{7,3},{1,5},{3,7},{12,8},{14,10},{8,... | collective-permute-start | bytes 589832 | tf_op jit(solution)/shard_map/ppermute | solution.py:338
  12.3 4.9 %collective-permute-start.3 = (s32[8,16]{1,0:T(8,128)S(1)}, s32[8,16]{1,0:T(8,128)S(1)}, u32[]{:S(2)}, u32[]{:S(2)}) collective-permute-start(s32[8,16]{1,0:T(8,128)S(1)} %copy-done.8), channel_id=1, source_target_pairs={{0,2},{2,0},{4,6},{6,4},{1,3},{3,1},{5,7},{7,5},{8,10},{10,8},{12,... | collective-permute-start | bytes 1544 | tf_op jit(solution)/shard_map/ppermute | solution.py:335
  17.5 17.6 %collective-permute-start.4 = (bf16[96,1024]{1,0:T(8,128)(2,1)S(1)}, bf16[96,1024]{1,0:T(8,128)(2,1)S(1)}, u32[]{:S(2)}, u32[]{:S(2)}) collective-permute-start(bf16[96,1024]{1,0:T(8,128)(2,1)S(1)} %shard_map.70), channel_id=1, source_target_pairs={{2,0},{0,2},{6,4},{4,6},{3,1},{1,3},{7,5},{5,7},{10,8},{8,10},{14,... | collective-permute-start | bytes 589832 | tf_op jit(solution)/shard_map/ppermute | solution.py:338
  20.1 7.7 %collective-permute-start.1 = (s32[8,16]{1,0:T(8,128)S(1)}, s32[8,16]{1,0:T(8,128)S(1)}, u32[]{:S(2)}, u32[]{:S(2)}) collective-permute-start(s32[8,16]{1,0:T(8,128)S(1)} %copy-done.8), channel_id=1, source_target_pairs={{0,6},{2,4},{4,2},{6,0},{1,7},{3,5},{5,3},{7,1},{8,14},{10,12},{12... | collective-permute-start | bytes 1544 | tf_op jit(solution)/shard_map/ppermute | solution.py:335
  28.0 8.6 %collective-permute-start.8 = (bf16[96,512]{1,0:T(8,128)(2,1)S(1)}, bf16[96,512]{1,0:T(8,128)(2,1)S(1)}, u32[]{:S(2)}, u32[]{:S(2)}) collective-permute-start(bf16[96,512]{1,0:T(8,128)(2,1)S(1)} %get-tuple-element.34), channel_id=1, source_target_pairs={{6,0},{4,2},{2,4},{0,6},{7,1},{5,3},{3,5},{1,7},{14,8},{12,10},{10... | collective-permute-start | bytes 294920 | tf_op jit(solution)/shard_map/ppermute | solution.py:338
  29.5 6.4 %collective-permute-start.2 = (bf16[96,512]{1,0:T(8,128)(2,1)S(1)}, bf16[96,512]{1,0:T(8,128)(2,1)S(1)}, u32[]{:S(2)}, u32[]{:S(2)}) collective-permute-start(bf16[96,512]{1,0:T(8,128)(2,1)S(1)} %get-tuple-element.23), channel_id=1, source_target_pairs={{6,0},{4,2},{2,4},{0,6},{7,1},{5,3},{3,5},{1,7},{14,8},{12,10},{10... | collective-permute-start | bytes 294920 | tf_op jit(solution)/shard_map/ppermute | solution.py:338
  34.5 3.4 %copy-start = (bf16[1024,1024]{1,0:T(8,128)(2,1)S(1)}, bf16[1024,1024]{1,0:T(8,128)(2,1)}, u32[]{:S(2)}) copy-start(bf16[1024,1024]{1,0:T(8,128)(2,1)} %weight_ref.7) | copy-start | bytes 6291460
  36.5 1.4 %collective-permute-start.7 = (bf16[256,256]{1,0:T(8,128)(2,1)S(1)}, bf16[256,256]{1,0:T(8,128)(2,1)S(1)}, u32[]{:S(2)}, u32[]{:S(2)}) collective-permute-start(bf16[256,256]{1,0:T(8,128)(2,1)S(1)} %shard_map.75.own_ref), channel_id=1, source_target_pairs={{0,1},{1,0},{2,3},{3,2},{4,5},{5,4},{6,7},{7,6},{8,9},{9,8},{10,11... | collective-permute-start | bytes 393224 | tf_op jit(solution)/shard_map/ppermute | solution.py:411
  37.1 1.5 %collective-permute-start.9 = (bf16[256,256]{1,0:T(8,128)(2,1)S(1)}, bf16[256,256]{1,0:T(8,128)(2,1)S(1)}, u32[]{:S(2)}, u32[]{:S(2)}) collective-permute-start(bf16[256,256]{1,0:T(8,128)(2,1)S(1)} %shard_map.77.own_ref), channel_id=1, source_target_pairs={{0,1},{1,0},{2,3},{3,2},{4,5},{5,4},{6,7},{7,6},{8,9},{9,8},{10,11... | collective-permute-start | bytes 393224 | tf_op jit(solution)/shard_map/ppermute | solution.py:411

commit v4 on v3

--- a/solution.py
+++ b/solution.py
@@ -335,7 +335,10 @@
         return lax.ppermute(x, "kv", [(i, source_of(i, turn, devices)) for i in range(devices)])
 
     def send(x, turn):
-        return lax.ppermute(x, "kv", [(source_of(i, turn, devices), i) for i in range(devices)])
+        pairs = [(source_of(i, turn, devices), i) for i in range(devices)]
+        if turn == turns[-1]:
+            pairs = [pair for pair in pairs if pair[0] < pair[1]]
+        return lax.ppermute(x, "kv", pairs)
 
     other = lax.ppermute(tokens, "tp", swap)
     asked, turns = [], turn_order(devices)

time: 40 us -> 40.7 us (1.018)
  starting transfers between devices: 16.7 us -> 17.5 us
    ppermute x4, starting transfers between devices: 6.51 us -> 7.29 us  [send(): return lax.ppermute(x, 'kv', pairs)]
  transfers between devices with their start and end apart: 10 -> 10, of which waited for: 4 -> 3; matrix products, arithmetic and copies ran while one was open for 0% -> 0% of each run, Pallas kernels for 22% -> 22%
where the time goes in v4:
time: 40.7 us; the launch traced here: 40.4 us
  starting transfers between devices  17.5 us (43%)
  Pallas kernels  10 us (25%)
  local copies, waits for them, and re-layouts  6.31 us (16%)
  waiting for transfers between devices  6.29 us (15%)
    pallas_call x16, Pallas kernels, call(): pl.pallas_call(kernel, in_specs=[VMEM] * near + [anywhere] * far, out_spe...  10 us
    ppermute x3, starting transfers between devices, ask(): lax.ppermute(x, 'kv', [(i, source_of(i, turn, devices)) for i in range(de...  9.12 us
    ppermute x4, starting transfers between devices, send(): return lax.ppermute(x, 'kv', pairs)  7.29 us
    unnamed x18, local copies, waits for them, and re-layouts  6.31 us
    ppermute x3, waiting for transfers between devices, ask(): lax.ppermute(x, 'kv', [(i, source_of(i, turn, devices)) for i in range(de...  6.05 us
  transfers between devices with their start and end apart: 10, of which 3 were waited for; matrix products, arithmetic and copies ran while one was open for 0% of the time, Pallas kernels for 22%

profile of v4, /device:TPU:0, one launch (start us, length us, event | category | flops | bytes accessed | tf_op | source)
XLA Modules:
  0.0 40.4 jit_solution(9354980815237477122)
XLA Ops:
  0.5 3.6 %collective-permute-start.5 = (s32[8,16]{1,0:T(8,128)}, s32[8,16]{1,0:T(8,128)S(1)}, u32[]{:S(2)}, u32[]{:S(2)}) collective-permute-start(s32[8,16]{1,0:T(8,128)} %far_ref.1), channel_id=1, source_target_pairs={{0,4},{2,6},{4,0},{6,2},{1,5},{3,7},{5,1},{7,3},{8,12},{10,14},{12... | collective-permute-start | bytes 1544 | tf_op jit(solution)/shard_map/ppermute | solution.py:335
  4.1 1.6 %copy-done.1 = bf16[2048,512]{1,0:T(8,128)(2,1)S(1)} copy-done((bf16[2048,512]{1,0:T(8,128)(2,1)S(1)}, bf16[2048,512]{1,0:T(8,128)(2,1)}, u32[]{:S(2)}) %copy-start.1) | copy-done | bytes 2097176
  5.7 1.6 %copy-done.3 = bf16[2048,512]{1,0:T(8,128)(2,1)S(1)} copy-done((bf16[2048,512]{1,0:T(8,128)(2,1)S(1)}, bf16[2048,512]{1,0:T(8,128)(2,1)}, u32[]{:S(2)}) %copy-start.3) | copy-done | bytes 2097176
  7.3 1.0 %copy-done.6 = bf16[256,1024]{1,0:T(8,128)(2,1)S(1)} copy-done((bf16[256,1024]{1,0:T(8,128)(2,1)S(1)}, bf16[256,1024]{1,0:T(8,128)(2,1)}, u32[]{:S(2)}) %copy-start.6) | copy-done | bytes 524312
  8.3 0.7 %shard_map.67.part_ref = f32[256,1024]{1,0:T(8,128)S(1)} custom-call(bf16[256,1024]{1,0:T(8,128)(2,1)S(1)} %copy-done.6, bf16[2048,512]{1,0:T(8,128)(2,1)S(1)} %copy-done.1, bf16[2048,512]{1,0:T(8,128)(2,1)S(1)} %copy-done.3), custom_call_target="tpu_custom_call" | custom-call | flops 536870912 | bytes 100000 | tf_op jit(solution)/shard_map/pallas_call | solution.py:38
  9.2 1.4 %copy-done.2 = bf16[2048,512]{1,0:T(8,128)(2,1)S(1)} copy-done((bf16[2048,512]{1,0:T(8,128)(2,1)S(1)}, bf16[2048,512]{1,0:T(8,128)(2,1)}, u32[]{:S(2)}) %copy-start.2) | copy-done | bytes 2097176
  10.6 0.6 %copy-done.4 = bf16[2048,512]{1,0:T(8,128)(2,1)S(1)} copy-done((bf16[2048,512]{1,0:T(8,128)(2,1)S(1)}, bf16[2048,512]{1,0:T(8,128)(2,1)}, u32[]{:S(2)}) %copy-start.4) | copy-done | bytes 2097176
  11.2 0.7 %shard_map.68.store_ref = bf16[256,1024]{1,0:T(8,128)(2,1)S(1)} custom-call(f32[256,1024]{1,0:T(8,128)S(1)} %shard_map.67.part_ref, bf16[256,1024]{1,0:T(8,128)(2,1)S(1)} %collective-permute-done.other_ref, bf16[2048,512]{1,0:T(8,128)(2,1)S(1)} %copy-done.2, bf16[2048,512]{1,0:T(8,128)(2,1)S(1)} %copy-done.4, f32[256,128]{1,0:T(8,128)S(1)} %get-tuple-element.20.cos_ref, ...), custom_call_target="tpu_custom_call" | custom-call | flops 536870912 | bytes 100000 | tf_op jit(solution)/shard_map/pallas_call | solution.py:38
  12.3 1.9 %collective-permute-start.3 = (s32[8,16]{1,0:T(8,128)S(1)}, s32[8,16]{1,0:T(8,128)S(1)}, u32[]{:S(2)}, u32[]{:S(2)}) collective-permute-start(s32[8,16]{1,0:T(8,128)S(1)} %copy-done.8), channel_id=1, source_target_pairs={{0,2},{2,0},{4,6},{6,4},{1,3},{3,1},{5,7},{7,5},{8,10},{10,8},{12,... | collective-permute-start | bytes 1544 | tf_op jit(solution)/shard_map/ppermute | solution.py:335
  14.2 3.1 %collective-permute-done.3.asked_ref = s32[8,16]{1,0:T(8,128)S(1)} collective-permute-done((s32[8,16]{1,0:T(8,128)S(1)}, s32[8,16]{1,0:T(8,128)S(1)}, u32[]{:S(2)}, u32[]{:S(2)}) %collective-permute-start.3) | collective-permute-done | bytes 544 | tf_op jit(solution)/shard_map/ppermute | solution.py:335
  17.5 2.5 %collective-permute-start.4 = (bf16[96,1024]{1,0:T(8,128)(2,1)S(1)}, bf16[96,1024]{1,0:T(8,128)(2,1)S(1)}, u32[]{:S(2)}, u32[]{:S(2)}) collective-permute-start(bf16[96,1024]{1,0:T(8,128)(2,1)S(1)} %shard_map.70), channel_id=1, source_target_pairs={{2,0},{0,2},{6,4},{4,6},{3,1},{1,3},{7,5},{5,7},{10,8},{8,10},{14,... | collective-permute-start | bytes 589832 | tf_op jit(solution)/shard_map/ppermute | solution.py:341
  20.1 3.7 %collective-permute-start.1 = (s32[8,16]{1,0:T(8,128)S(1)}, s32[8,16]{1,0:T(8,128)S(1)}, u32[]{:S(2)}, u32[]{:S(2)}) collective-permute-start(s32[8,16]{1,0:T(8,128)S(1)} %copy-done.8), channel_id=1, source_target_pairs={{0,6},{2,4},{4,2},{6,0},{1,7},{3,5},{5,3},{7,1},{8,14},{10,12},{12... | collective-permute-start | bytes 1544 | tf_op jit(solution)/shard_map/ppermute | solution.py:335
  23.7 1.0 %shard_map.66 = (f32[8,256]{1,0:T(8,128)S(1)}, f32[9,256]{1,0:T(8,128)S(1)}) custom-call(s32[8,16]{1,0:T(8,128)} %far_ref.1), custom_call_target="tpu_custom_call" | custom-call | flops 1000000 | bytes 100000 | tf_op jit(solution)/shard_map/pallas_call | solution.py:38
  24.8 3.0 %collective-permute-done.1.asked_ref = s32[8,16]{1,0:T(8,128)S(1)} collective-permute-done((s32[8,16]{1,0:T(8,128)S(1)}, s32[8,16]{1,0:T(8,128)S(1)}, u32[]{:S(2)}, u32[]{:S(2)}) %collective-permute-start.1) | collective-permute-done | bytes 544 | tf_op jit(solution)/shard_map/ppermute | solution.py:335
  28.0 3.4 %collective-permute-start.8 = (bf16[96,512]{1,0:T(8,128)(2,1)S(1)}, bf16[96,512]{1,0:T(8,128)(2,1)S(1)}, u32[]{:S(2)}, u32[]{:S(2)}) collective-permute-start(bf16[96,512]{1,0:T(8,128)(2,1)S(1)} %get-tuple-element.34), channel_id=1, source_target_pairs={{2,4},{0,6},{3,5},{1,7},{10,12},{8,14},{11,13},{9,15},{18,20},{16,... | collective-permute-start | bytes 294920 | tf_op jit(solution)/shard_map/ppermute | solution.py:341
  31.4 1.3 %collective-permute-start.2 = (bf16[96,512]{1,0:T(8,128)(2,1)S(1)}, bf16[96,512]{1,0:T(8,128)(2,1)S(1)}, u32[]{:S(2)}, u32[]{:S(2)}) collective-permute-start(bf16[96,512]{1,0:T(8,128)(2,1)S(1)} %get-tuple-element.23), channel_id=1, source_target_pairs={{2,4},{0,6},{3,5},{1,7},{10,12},{8,14},{11,13},{9,15},{18,20},{16,... | collective-permute-start | bytes 294920 | tf_op jit(solution)/shard_map/ppermute | solution.py:341
  32.7 1.0 %shard_map.65.query_ref = bf16[256,512]{1,0:T(8,128)(2,1)S(1)} custom-call(bf16[256,1024]{1,0:T(8,128)(2,1)S(1)} %copy-done.7, bf16[256,1024]{1,0:T(8,128)(2,1)S(1)} %collective-permute-done.other_ref, bf16[2048,512]{1,0:T(8,128)(2,1)S(1)} %copy-done.5, f32[256,128]{1,0:T(8,128)S(1)} %get-tuple-element.20.cos_ref, f32[256,128]{1,0:T(8,128)S(1)} %get-tuple-element.21.sin_ref), custom_call_target="tpu_custom_call" | custom-call | flops 536870912 | bytes 100000 | tf_op jit(solution)/shard_map/pallas_call | solution.py:38
  33.7 1.6 %shard_map.72 = (f32[4,512]{1,0:T(4,128)S(1)}, f32[4,512]{1,0:T(4,128)S(1)}, f32[512,256]{1,0:T(8,128)S(1)}) custom-call(bf16[256,512]{1,0:T(8,128)(2,1)S(1)} %shard_map.65.query_ref, bf16[256,1024]{1,0:T(8,128)(2,1)S(1)} %shard_map.68.store_ref, f32[8,256]{1,0:T(8,128)S(1)} %get-tuple-element.24.bias_ref), custom_call_target="tpu_custom_call" | custom-call | flops 536870912 | bytes 100000 | tf_op jit(solution)/shard_map/pallas_call | solution.py:38
  35.3 0.6 %shard_map.73 = (f32[4,512]{1,0:T(4,128)S(1)}, f32[4,512]{1,0:T(4,128)S(1)}, f32[512,256]{1,0:T(8,128)S(1)}) custom-call(bf16[256,512]{1,0:T(8,128)(2,1)S(1)} %shard_map.65.query_ref, f32[9,256]{1,0:T(8,128)S(1)} %get-tuple-element.22.bias_ref, bf16[96,1024]{1,0:T(8,128)(2,1)S(1)} %collective-permute-done.6.got_ref, f32[4,512]{1,0:T(4,128)S(1)} %get-tuple-element.25.refs_0_, ...), custom_call_target="tpu_custom_call" | custom-call | flops 201326592 | bytes 100000 | tf_op jit(solution)/shard_map/pallas_call | solution.py:38
  36.0 0.6 %shard_map.74 = (f32[4,512]{1,0:T(4,128)S(1)}, f32[4,512]{1,0:T(4,128)S(1)}, f32[512,256]{1,0:T(8,128)S(1)}) custom-call(bf16[256,512]{1,0:T(8,128)(2,1)S(1)} %shard_map.65.query_ref, f32[9,256]{1,0:T(8,128)S(1)} %get-tuple-element.22.bias_ref, bf16[96,1024]{1,0:T(8,128)(2,1)S(1)} %collective-permute-done.4.got_ref, f32[4,512]{1,0:T(4,128)S(1)} %get-tuple-element.28.refs_0_, ...), custom_call_target="tpu_custom_call" | custom-call | flops 201326592 | bytes 100000 | tf_op jit(solution)/shard_map/pallas_call | solution.py:38
  36.6 0.5 %shard_map.75.own_ref = bf16[256,256]{1,0:T(8,128)(2,1)S(1)} custom-call(bf16[256,512]{1,0:T(8,128)(2,1)S(1)} %shard_map.65.query_ref, f32[9,256]{1,0:T(8,128)S(1)} %get-tuple-element.22.bias_ref, bf16[96,512]{1,0:T(8,128)(2,1)S(1)} %collective-permute-done.2.got_ref, f32[4,512]{1,0:T(4,128)S(1)} %get-tuple-element.31.refs_0_, ...), custom_call_target="tpu_custom_call" | custom-call | flops 100663296 | bytes 100000 | tf_op jit(solution)/shard_map/pallas_call | solution.py:38
  37.2 0.5 %shard_map.77.own_ref = bf16[256,256]{1,0:T(8,128)(2,1)S(1)} custom-call(bf16[256,512]{1,0:T(8,128)(2,1)S(1)} %shard_map.65.query_ref, f32[9,256]{1,0:T(8,128)S(1)} %get-tuple-element.22.bias_ref, bf16[96,512]{1,0:T(8,128)(2,1)S(1)} %collective-permute-done.8.got_ref, f32[4,512]{1,0:T(4,128)S(1)} %get-tuple-element.31.refs_0_, ...), custom_call_target="tpu_custom_call" | custom-call | flops 100663296 | bytes 100000 | tf_op jit(solution)/shard_map/pallas_call | solution.py:38
  37.8 0.6 %collective-permute-start.9 = (bf16[256,256]{1,0:T(8,128)(2,1)S(1)}, bf16[256,256]{1,0:T(8,128)(2,1)S(1)}, u32[]{:S(2)}, u32[]{:S(2)}) collective-permute-start(bf16[256,256]{1,0:T(8,128)(2,1)S(1)} %shard_map.77.own_ref), channel_id=1, source_target_pairs={{0,1},{1,0},{2,3},{3,2},{4,5},{5,4},{6,7},{7,6},{8,9},{9,8},{10,11... | collective-permute-start | bytes 393224 | tf_op jit(solution)/shard_map/ppermute | solution.py:414
  39.3 1.1 %shard_map.79 = bf16[256,1024]{1,0:T(8,128)(2,1)} custom-call(f32[256,1024]{1,0:T(8,128)S(1)} %shard_map.78.part_ref, bf16[256,256]{1,0:T(8,128)(2,1)S(1)} %collective-permute-done.9.other_ref, bf16[1024,1024]{1,0:T(8,128)(2,1)S(1)} %copy-done), custom_call_target="tpu_custom_call" | custom-call | flops 134217728 | bytes 100000 | tf_op jit(solution)/shard_map/pallas_call | solution.py:38
  (30 shorter events, 2.5 us)
Async XLA Ops:
  0.0 9.2 %collective-permute-start = (bf16[256,1024]{1,0:T(8,128)(2,1)}, bf16[256,1024]{1,0:T(8,128)(2,1)S(1)}, u32[]{:S(2)}, u32[]{:S(2)}) collective-permute-start(bf16[256,1024]{1,0:T(8,128)(2,1)} %own_ref.3), channel_id=1, source_target_pairs={{0,1},{1,0},{2,3},{3,2},{4,5},{5,4},{6,7},{7,6},{8,9},{9,8},{10,11... | collective-permute-start | bytes 1572872 | tf_op jit(solution)/shard_map/ppermute | solution.py:343
  0.5 11.5 %collective-permute-start.5 = (s32[8,16]{1,0:T(8,128)}, s32[8,16]{1,0:T(8,128)S(1)}, u32[]{:S(2)}, u32[]{:S(2)}) collective-permute-start(s32[8,16]{1,0:T(8,128)} %far_ref.1), channel_id=1, source_target_pairs={{0,4},{2,6},{4,0},{6,2},{1,5},{3,7},{5,1},{7,3},{8,12},{10,14},{12... | collective-permute-start | bytes 1544 | tf_op jit(solution)/shard_map/ppermute | solution.py:335
  4.1 1.6 %copy-start.1 = (bf16[2048,512]{1,0:T(8,128)(2,1)S(1)}, bf16[2048,512]{1,0:T(8,128)(2,1)}, u32[]{:S(2)}) copy-start(bf16[2048,512]{1,0:T(8,128)(2,1)} %key_ref.3) | copy-start | bytes 6291460
  5.7 1.6 %copy-start.3 = (bf16[2048,512]{1,0:T(8,128)(2,1)S(1)}, bf16[2048,512]{1,0:T(8,128)(2,1)}, u32[]{:S(2)}) copy-start(bf16[2048,512]{1,0:T(8,128)(2,1)} %value_ref.3) | copy-start | bytes 6291460
  7.3 1.0 %copy-start.6 = (bf16[256,1024]{1,0:T(8,128)(2,1)S(1)}, bf16[256,1024]{1,0:T(8,128)(2,1)}, u32[]{:S(2)}) copy-start(bf16[256,1024]{1,0:T(8,128)(2,1)} %own_ref.3) | copy-start | bytes 1572868
  9.0 1.6 %copy-start.2 = (bf16[2048,512]{1,0:T(8,128)(2,1)S(1)}, bf16[2048,512]{1,0:T(8,128)(2,1)}, u32[]{:S(2)}) copy-start(bf16[2048,512]{1,0:T(8,128)(2,1)} %key_ref.3) | copy-start | bytes 6291460
  9.0 2.2 %copy-start.4 = (bf16[2048,512]{1,0:T(8,128)(2,1)S(1)}, bf16[2048,512]{1,0:T(8,128)(2,1)}, u32[]{:S(2)}) copy-start(bf16[2048,512]{1,0:T(8,128)(2,1)} %value_ref.3) | copy-start | bytes 6291460
  11.2 1.1 %copy-start.8 = (s32[8,16]{1,0:T(8,128)S(1)}, s32[8,16]{1,0:T(8,128)}, u32[]{:S(2)}) copy-start(s32[8,16]{1,0:T(8,128)} %far_ref.1) | copy-start | bytes 1540
  11.2 21.5 %copy-start.5 = (bf16[2048,512]{1,0:T(8,128)(2,1)S(1)}, bf16[2048,512]{1,0:T(8,128)(2,1)}, u32[]{:S(2)}) copy-start(bf16[2048,512]{1,0:T(8,128)(2,1)} %weight_ref.4) | copy-start | bytes 6291460
  12.0 20.7 %copy-start.7 = (bf16[256,1024]{1,0:T(8,128)(2,1)S(1)}, bf16[256,1024]{1,0:T(8,128)(2,1)}, u32[]{:S(2)}) copy-start(bf16[256,1024]{1,0:T(8,128)(2,1)} %own_ref.3) | copy-start | bytes 1572868
  12.2 23.1 %collective-permute-start.6 = (bf16[96,1024]{1,0:T(8,128)(2,1)S(1)}, bf16[96,1024]{1,0:T(8,128)(2,1)S(1)}, u32[]{:S(2)}, u32[]{:S(2)}) collective-permute-start(bf16[96,1024]{1,0:T(8,128)(2,1)S(1)} %shard_map.71), channel_id=1, source_target_pairs={{4,0},{6,2},{0,4},{2,6},{5,1},{7,3},{1,5},{3,7},{12,8},{14,10},{8,... | collective-permute-start | bytes 589832 | tf_op jit(solution)/shard_map/ppermute | solution.py:341
  12.3 4.9 %collective-permute-start.3 = (s32[8,16]{1,0:T(8,128)S(1)}, s32[8,16]{1,0:T(8,128)S(1)}, u32[]{:S(2)}, u32[]{:S(2)}) collective-permute-start(s32[8,16]{1,0:T(8,128)S(1)} %copy-done.8), channel_id=1, source_target_pairs={{0,2},{2,0},{4,6},{6,4},{1,3},{3,1},{5,7},{7,5},{8,10},{10,8},{12,... | collective-permute-start | bytes 1544 | tf_op jit(solution)/shard_map/ppermute | solution.py:335
  17.5 18.4 %collective-permute-start.4 = (bf16[96,1024]{1,0:T(8,128)(2,1)S(1)}, bf16[96,1024]{1,0:T(8,128)(2,1)S(1)}, u32[]{:S(2)}, u32[]{:S(2)}) collective-permute-start(bf16[96,1024]{1,0:T(8,128)(2,1)S(1)} %shard_map.70), channel_id=1, source_target_pairs={{2,0},{0,2},{6,4},{4,6},{3,1},{1,3},{7,5},{5,7},{10,8},{8,10},{14,... | collective-permute-start | bytes 589832 | tf_op jit(solution)/shard_map/ppermute | solution.py:341
  20.1 7.7 %collective-permute-start.1 = (s32[8,16]{1,0:T(8,128)S(1)}, s32[8,16]{1,0:T(8,128)S(1)}, u32[]{:S(2)}, u32[]{:S(2)}) collective-permute-start(s32[8,16]{1,0:T(8,128)S(1)} %copy-done.8), channel_id=1, source_target_pairs={{0,6},{2,4},{4,2},{6,0},{1,7},{3,5},{5,3},{7,1},{8,14},{10,12},{12... | collective-permute-start | bytes 1544 | tf_op jit(solution)/shard_map/ppermute | solution.py:335
  28.0 9.2 %collective-permute-start.8 = (bf16[96,512]{1,0:T(8,128)(2,1)S(1)}, bf16[96,512]{1,0:T(8,128)(2,1)S(1)}, u32[]{:S(2)}, u32[]{:S(2)}) collective-permute-start(bf16[96,512]{1,0:T(8,128)(2,1)S(1)} %get-tuple-element.34), channel_id=1, source_target_pairs={{2,4},{0,6},{3,5},{1,7},{10,12},{8,14},{11,13},{9,15},{18,20},{16,... | collective-permute-start | bytes 294920 | tf_op jit(solution)/shard_map/ppermute | solution.py:341
  31.4 5.2 %collective-permute-start.2 = (bf16[96,512]{1,0:T(8,128)(2,1)S(1)}, bf16[96,512]{1,0:T(8,128)(2,1)S(1)}, u32[]{:S(2)}, u32[]{:S(2)}) collective-permute-start(bf16[96,512]{1,0:T(8,128)(2,1)S(1)} %get-tuple-element.23), channel_id=1, source_target_pairs={{2,4},{0,6},{3,5},{1,7},{10,12},{8,14},{11,13},{9,15},{18,20},{16,... | collective-permute-start | bytes 294920 | tf_op jit(solution)/shard_map/ppermute | solution.py:341
  35.3 3.3 %copy-start = (bf16[1024,1024]{1,0:T(8,128)(2,1)S(1)}, bf16[1024,1024]{1,0:T(8,128)(2,1)}, u32[]{:S(2)}) copy-start(bf16[1024,1024]{1,0:T(8,128)(2,1)} %weight_ref.7) | copy-start | bytes 6291460
  37.2 1.4 %collective-permute-start.7 = (bf16[256,256]{1,0:T(8,128)(2,1)S(1)}, bf16[256,256]{1,0:T(8,128)(2,1)S(1)}, u32[]{:S(2)}, u32[]{:S(2)}) collective-permute-start(bf16[256,256]{1,0:T(8,128)(2,1)S(1)} %shard_map.75.own_ref), channel_id=1, source_target_pairs={{0,1},{1,0},{2,3},{3,2},{4,5},{5,4},{6,7},{7,6},{8,9},{9,8},{10,11... | collective-permute-start | bytes 393224 | tf_op jit(solution)/shard_map/ppermute | solution.py:414
  37.8 1.5 %collective-permute-start.9 = (bf16[256,256]{1,0:T(8,128)(2,1)S(1)}, bf16[256,256]{1,0:T(8,128)(2,1)S(1)}, u32[]{:S(2)}, u32[]{:S(2)}) collective-permute-start(bf16[256,256]{1,0:T(8,128)(2,1)S(1)} %shard_map.77.own_ref), channel_id=1, source_target_pairs={{0,1},{1,0},{2,3},{3,2},{4,5},{5,4},{6,7},{7,6},{8,9},{9,8},{10,11... | collective-permute-start | bytes 393224 | tf_op jit(solution)/shard_map/ppermute | solution.py:414
